TPU v7x, 256 devices: a whole 4x4x8 slice. The times are simulated.
256 devices in a mesh: sp: 32 (over z, y), tp: 8 (over x, core).
Axes of the slice: x: 4, y: 4, z: 8, core: 2. Of those that a mesh axis runs over, the one named last changes fastest.
Arguments:
- grouped_head_inputs: bfloat16 [32768, 2, 1024], P('sp', None, 'tp'), may hold values from -6 to 6
- head_gate_inputs: bfloat16 [32768, 2, 1024], P('sp', None, 'tp'), may hold values from -6 to 6
- unsmoothed_step: float32 [32768, 2, 16], P('sp', None, 'tp'), may hold values from -3.8 to 3.8
- head_decay_rate: float32 [2, 16], P(None, 'tp'), may hold values from 3.0517578e-06 to 0.04761905
- extra_log_decay: float32 [32768, 2, 16], P('sp', None, 'tp'), may hold values from -1.4 to 0
- first_group_keys: bfloat16 [32768, 128], P('sp'), may hold values from -6 to 6
- first_group_queries: bfloat16 [32768, 128], P('sp'), may hold values from -6 to 6
- second_group_keys: bfloat16 [32768, 64], P('sp'), may hold values from -6 to 6
- second_group_queries: bfloat16 [32768, 64], P('sp'), may hold values from -6 to 6
- head_input_filter: float32 [4, 2, 1024], P(None, None, 'tp'), may hold values from -3 to 3
- first_group_filter: float32 [4, 2, 128], replicated, may hold values from -3 to 3
- second_group_filter: float32 [4, 2, 64], replicated, may hold values from -3 to 3
- head_norm_gain: float32 [2, 1024], P(None, 'tp'), may hold values from 0.1 to 1.9
- output_weight: bfloat16 [2, 1024, 2048], P(None, None, 'tp'), may hold values from -0.125 to 0.125
- residual: bfloat16 [32768, 2048], P('sp', 'tp'), may hold values from -37 to 37
- channel_norm_gain: float32 [2048], replicated, may hold values from 0.1 to 1.9
- channel_gate_weight: bfloat16 [2048, 5120], P('sp', 'tp'), may hold values from -0.125 to 0.125
- channel_up_weight: bfloat16 [2048, 5120], P('sp', 'tp'), may hold values from -0.125 to 0.125
- channel_down_weight: bfloat16 [2048, 5120], P('sp', 'tp'), may hold values from -0.078125 to 0.078125
Outputs:
- layer_output: bfloat16 [32768, 2048], P('sp', 'tp')
All inputs are finite; a program needn't handle non-finite values.
Results may differ from a plain program's by a relative error of at most 0.007.
Values may be sent and summed in bfloat16 or wider, within the bound.
No kernel may reach another device: no remote copies, remote signals or barrier semaphores. Data moves between devices by JAX's collectives and lax.ppermute only.
A program may use at most 128 MiB of HBM per device.

v0:
```python
import jax
import jax.numpy as jnp
from jax import lax
from jax.experimental import pallas as pl
from jax.experimental.pallas import tpu as pltpu
from jax.sharding import Mesh, PartitionSpec as P


EPSILON = 1e-06
BLOCK = 128
F32 = jnp.float32
BF16 = jnp.bfloat16
SP = ("z", "y")
TP = ("x", "c")


def silu(v):
    return v * jax.nn.sigmoid(v)


def shape(dims, kind):
    return jax.ShapeDtypeStruct(dims, kind)


def pack_rim_body(x_ref, k1_ref, q1_ref, k2_ref, q2_ref, out_ref):
    out_ref[:, 0:256] = x_ref[...]
    out_ref[:, 256:384] = k1_ref[...]
    out_ref[:, 384:512] = q1_ref[...]
    both = jnp.concatenate([k2_ref[...], q2_ref[...]], axis=0).astype(F32)
    out_ref[:, 512:640] = both.T[112:128].astype(BF16)


def pack_rim(x_flat, k1, q1, k2t, q2t):
    rows = k1.shape[0] // 16 - 1
    cols = k2t.shape[1] // 128 - 1
    return pl.pallas_call(
        pack_rim_body,
        grid=(1,),
        in_specs=[
            pl.BlockSpec((16, 256), lambda i: (rows, 0)),
            pl.BlockSpec((16, 128), lambda i: (rows, 0)),
            pl.BlockSpec((16, 128), lambda i: (rows, 0)),
            pl.BlockSpec((64, 128), lambda i: (0, cols)),
            pl.BlockSpec((64, 128), lambda i: (0, cols)),
        ],
        out_specs=pl.BlockSpec((16, 640), lambda i: (0, 0)),
        out_shape=shape((16, 640), BF16),
        name="pack_rim",
    )(x_flat, k1, q1, k2t, q2t)


def lanes_of(rows):
    return lax.broadcasted_iota(jnp.int32, (rows, 128), 1) < 64


def three_parts(v):
    hi = v.astype(BF16)
    rest = v - hi.astype(F32)
    mid = rest.astype(BF16)
    low = (rest - mid.astype(F32)).astype(BF16)
    return hi.astype(F32), mid.astype(F32), low.astype(F32)


def states_body(
    rate_ref, x_ref, k1_ref, q1_ref, k2_ref, q2_ref, rim_ref, fx_ref, f1_ref, f2_ref, step_ref,
    extra_ref,
    xc_ref, k1c_ref, q1c_ref, kq2c_ref, cum_ref, sp_ref, s1_ref, s2_ref, lead_ref, end_ref,
    buf, filt, raw, more,
):
    length = x_ref.shape[0]
    blocks = length // BLOCK
    upper = (
        lax.broadcasted_iota(jnp.int32, (BLOCK, BLOCK), 0)
        <= lax.broadcasted_iota(jnp.int32, (BLOCK, BLOCK), 1)
    ).astype(F32)
    raw[...] = jnp.zeros(raw.shape, F32)
    more[...] = jnp.zeros(more.shape, F32)
    for b in range(blocks):
        for head in range(4):
            row = b * 8 + head
            at = slice(b * BLOCK, (b + 1) * BLOCK)
            raw[row : row + 1, :] = step_ref[head // 2, head % 2 : head % 2 + 1, at]
            more[row : row + 1, :] = extra_ref[head // 2, head % 2 : head % 2 + 1, at]
    place = lax.broadcasted_iota(jnp.int32, (8, BLOCK), 0)
    rate = jnp.zeros((8, BLOCK), F32)
    for head in range(4):
        rate = jnp.where(place == head, rate_ref[head // 2, head % 2], rate)
    values = raw[...]
    soft = jnp.maximum(values, 0.0) + jnp.log1p(jnp.exp(-jnp.abs(values)))
    sp_ref[...] = soft
    logs = more[...] - soft * jnp.concatenate([rate] * blocks, axis=0)
    cum_ref[...] = jnp.dot(
        logs, upper, precision=lax.Precision.HIGHEST, preferred_element_type=F32
    )
    for k in range(4):
        filt[k : k + 1, 0:128] = fx_ref[k, 0:1, :]
        filt[k : k + 1, 128:256] = fx_ref[k, 1:2, :]
        filt[k : k + 1, 256:384] = f1_ref[k, 0:1, :]
        filt[k : k + 1, 384:512] = f1_ref[k, 1:2, :]
        filt[k : k + 1, 512:640] = jnp.concatenate([f2_ref[k, 0:1, :], f2_ref[k, 1:2, :]], axis=1)
    buf[0:8, :] = rim_ref[8:16, :].astype(F32)
    first = lanes_of(1)

    def fill(b, none):
        at = pl.ds(pl.multiple_of(b * BLOCK, BLOCK), BLOCK)
        to = pl.ds(pl.multiple_of(b * BLOCK + 8, 8), BLOCK)
        buf[to, 0:256] = x_ref[at, :].astype(F32)
        buf[to, 256:384] = k1_ref[at, :].astype(F32)
        buf[to, 384:512] = q1_ref[at, :].astype(F32)
        both = jnp.concatenate([k2_ref[:, at], q2_ref[:, at]], axis=0).astype(F32)
        buf[to, 512:640] = both.T
        return none

    def step(b, carry):
        state_one, state_two, lead_one, lead_two = carry
        fill(b, 0)
        at = pl.ds(pl.multiple_of(b * BLOCK, BLOCK), BLOCK)
        around = pl.ds(pl.multiple_of(b * BLOCK, BLOCK), BLOCK + 8)

        def conv(lo, hi):
            window = buf[around, lo:hi]
            run = filt[0:1, lo:hi] * window[5 : 5 + BLOCK]
            for k in range(1, 4):
                run = run + filt[k : k + 1, lo:hi] * window[5 + k : 5 + k + BLOCK]
            return silu(run)

        x_one = conv(0, 128).astype(BF16)
        x_two = conv(128, 256).astype(BF16)
        xc_ref[at, 0:128] = x_one
        xc_ref[at, 128:256] = x_two
        k_one = conv(256, 384)
        k1c_ref[at, :] = k_one.astype(BF16)
        q1c_ref[at, :] = conv(384, 512).astype(BF16)
        kq_two = conv(512, 640)
        kq2c_ref[at, :] = kq_two.astype(BF16)
        s1_ref[at, :] = state_one.astype(BF16)
        s2_ref[at, :] = jnp.concatenate(
            [jnp.zeros((64, 128), BF16), state_two.astype(BF16)], axis=0
        )
        eight = pl.ds(pl.multiple_of(b * 8, 8), 8)
        lead_ref[eight, :] = jnp.concatenate(
            [lead_one, lead_two, jnp.zeros((6, 128), F32)], axis=0
        )
        rows, softs = cum_ref[eight, :], sp_ref[eight, :]
        tot = rows[:, 127:128]
        weight = jnp.exp(tot - rows) * softs
        key_one = k_one.T
        key_two = kq_two.T[0:64]
        ups = [
            jnp.dot(
                ((key_one if head < 2 else key_two) * weight[head : head + 1, :]).astype(BF16),
                x_one if head < 2 else x_two,
                preferred_element_type=F32,
            )
            for head in range(4)
        ]
        wide = jnp.broadcast_to(tot, (8, 128))
        tot_one = jnp.where(first, wide[0:1], wide[1:2])
        tot_two = jnp.where(first, wide[2:3], wide[3:4])
        return (
            state_one * jnp.exp(tot_one) + jnp.where(first, ups[0], ups[1]),
            state_two * jnp.exp(tot_two) + jnp.where(first, ups[2], ups[3]),
            lead_one + tot_one,
            lead_two + tot_two,
        )

    state_one, state_two, lead_one, lead_two = lax.fori_loop(
        0,
        blocks,
        step,
        (
            jnp.zeros((128, 128), F32),
            jnp.zeros((64, 128), F32),
            jnp.zeros((1, 128), F32),
            jnp.zeros((1, 128), F32),
        ),
    )
    end_ref[0:128, :] = state_one.astype(BF16)
    end_ref[128:192, :] = state_two.astype(BF16)
    end_ref[192:208, :] = log_rows(lead_one, lead_two)


def log_rows(one, two):
    parts = three_parts(one) + three_parts(two)
    return jnp.concatenate(list(parts) + [jnp.zeros((10, 128), F32)], axis=0).astype(BF16)


def logs_in(payload_ref):
    rows = payload_ref[192:208, :].astype(F32)
    one = rows[0:1] + rows[1:2] + rows[2:3]
    two = rows[3:4] + rows[4:5] + rows[5:6]
    return one, two


def inside_body(xc_ref, k1_ref, q1_ref, kq2_ref, cum_ref, sp_ref, out_ref):
    length = xc_ref.shape[0]
    causal = lax.broadcasted_iota(jnp.int32, (BLOCK, BLOCK), 0) >= lax.broadcasted_iota(
        jnp.int32, (BLOCK, BLOCK), 1
    )
    first = lanes_of(1)
    contract = (((1,), (1,)), ((), ()))

    def step(b, none):
        at = pl.ds(pl.multiple_of(b * BLOCK, BLOCK), BLOCK)
        eight = pl.ds(pl.multiple_of(b * 8, 8), 8)
        rows, softs = cum_ref[eight, :], sp_ref[eight, :]
        columns = rows.T
        kq_two = kq2_ref[at, :].astype(F32)
        query_two = jnp.where(first, 0.0, kq_two).astype(BF16)
        key_two = pltpu.roll(kq_two, 64, 1).astype(BF16)
        scores = (
            lax.dot_general(q1_ref[at, :], k1_ref[at, :], contract, preferred_element_type=F32),
            lax.dot_general(query_two, key_two, contract, preferred_element_type=F32),
        )
        for group in range(2):
            values = xc_ref[at, group * 128 : group * 128 + 128]
            parts = []
            for inner in range(2):
                h = group * 2 + inner
                spans = jnp.where(causal, columns[:, h : h + 1] - rows[h : h + 1, :], -jnp.inf)
                weights = jnp.exp(spans) * (scores[group] * softs[h : h + 1, :])
                parts.append(jnp.dot(weights.astype(BF16), values, preferred_element_type=F32))
            out_ref[at, group * 128 : group * 128 + 128] = jnp.where(first, parts[0], parts[1])
        return none

    lax.fori_loop(0, length // BLOCK, step, 0)


def combine_body(y_ref, own_ref, b1_ref, b2_ref, b3_ref, pre_ref, lead_ref, total_ref):
    y = y_ref[3]
    refs = (own_ref, b1_ref, b2_ref, b3_ref)
    place = [lax.rem(y - k + 4, 4) for k in range(4)]
    logs = [logs_in(r) for r in refs]
    zero = jnp.zeros((1, 128), F32)

    def pick(flag, v):
        return jnp.where(flag, v, zero)

    leads = [zero, zero]
    pre_one = jnp.zeros((128, 128), F32)
    pre_two = jnp.zeros((64, 128), F32)
    tot_one = jnp.zeros((128, 128), F32)
    tot_two = jnp.zeros((64, 128), F32)
    for k in range(4):
        one = refs[k][0:128, :].astype(F32)
        two = refs[k][128:192, :].astype(F32)
        if k:
            flag = k <= y
            pre_one = pre_one + pick(flag, jnp.exp(leads[0])) * one
            pre_two = pre_two + pick(flag, jnp.exp(leads[1])) * two
            leads = [leads[g] + pick(flag, logs[k][g]) for g in range(2)]
        later = [zero, zero]
        for j in range(4):
            if j != k:
                flag = place[j] > place[k]
                later = [later[g] + pick(flag, logs[j][g]) for g in range(2)]
        tot_one = tot_one + jnp.exp(later[0]) * one
        tot_two = tot_two + jnp.exp(later[1]) * two
    pre_ref[0:128, :] = pre_one
    pre_ref[128:192, :] = pre_two
    lead_ref[0:1, :] = leads[0]
    lead_ref[1:2, :] = leads[1]
    tot_one = tot_one.astype(BF16)
    tot_two = tot_two.astype(BF16)
    tot_logs = log_rows(
        logs[0][0] + logs[1][0] + logs[2][0] + logs[3][0],
        logs[0][1] + logs[1][1] + logs[2][1] + logs[3][1],
    )
    for z in range(total_ref.shape[0]):
        total_ref[z, 0:128, :] = tot_one
        total_ref[z, 128:192, :] = tot_two
        total_ref[z, 192:208, :] = tot_logs


def mixed_body(
    pos_ref, in_ref, gate_ref, q1_ref, kq2_ref, cum_ref, s1_ref, s2_ref, lead_ref, gain_ref,
    pre_ref, ylead_ref, rows_ref, mine_ref, theirs_ref,
):
    c, z = pos_ref[1], pos_ref[2]
    far_one = jnp.zeros((128, 128), F32)
    far_two = jnp.zeros((64, 128), F32)
    run = [jnp.zeros((1, 128), F32)] * 2
    for k in reversed(range(rows_ref.shape[0] - 1)):
        flag = k < z
        r = rows_ref.at[k]
        scale = [jnp.where(flag, jnp.exp(v), 0.0) for v in run]
        far_one = far_one + scale[0] * r[0:128, :].astype(F32)
        far_two = far_two + scale[1] * r[128:192, :].astype(F32)
        logs = logs_in(r)
        run = [v + jnp.where(flag, more, 0.0) for v, more in zip(run, logs)]
    enter = (
        pre_ref[0:128, :] + jnp.exp(ylead_ref[0:1, :]) * far_one,
        jnp.concatenate(
            [
                jnp.zeros((64, 128), F32),
                pre_ref[128:192, :] + jnp.exp(ylead_ref[1:2, :]) * far_two,
            ],
            axis=0,
        ),
    )
    first = lanes_of(1)
    same_head = (
        (lax.broadcasted_iota(jnp.int32, (128, 128), 0) < 64)
        == (lax.broadcasted_iota(jnp.int32, (128, 128), 1) < 64)
    ).astype(BF16)
    blocks = in_ref.shape[0] // BLOCK
    half = blocks // 2

    def block(b, out_ref, to):
        at = pl.ds(pl.multiple_of(b * BLOCK, BLOCK), BLOCK)
        eight = pl.ds(pl.multiple_of(b * 8, 8), 8)
        columns = jnp.exp(cum_ref[eight, :].T)
        leads = jnp.exp(lead_ref[eight, :])
        for group in range(2):
            lane = slice(group * 128, group * 128 + 128)
            states = (s1_ref, s2_ref)[group][at, :].astype(F32)
            state = (states + leads[group : group + 1, :] * enter[group]).astype(BF16)
            query = (q1_ref, kq2_ref)[group][at, :]
            h = group * 2
            decay = jnp.where(first, columns[:, h : h + 1], columns[:, h + 1 : h + 2])
            mixer = in_ref[at, lane] + decay * jnp.dot(
                query, state, preferred_element_type=F32
            )
            gated = mixer * silu(gate_ref[at, lane].astype(F32))
            square = gated * gated
            hi = square.astype(BF16)
            low = (square - hi.astype(F32)).astype(BF16)
            mean = (
                jnp.dot(hi, same_head, preferred_element_type=F32)
                + jnp.dot(low, same_head, preferred_element_type=F32)
            ) * (1.0 / 64.0)
            scaled = gated * lax.rsqrt(mean + EPSILON) * gain_ref[group : group + 1, :]
            out_ref[to, lane] = scaled.astype(BF16)

    def step(i, none):
        to = pl.ds(pl.multiple_of(i * BLOCK, BLOCK), BLOCK)
        block(c * half + i, mine_ref, to)
        block((1 - c) * half + i, theirs_ref, to)
        return none

    lax.fori_loop(0, half, step, 0)


def projection_body(pos_ref, *refs):
    chunk_refs, (w_ref, res_ref, a_ref, b_ref, lhs) = refs[:8], refs[8:]
    x, c = pos_ref[0], pos_ref[1]
    for j, shift in enumerate((0, -1, 1, 2)):
        there = lax.rem(x + shift + 4, 4)
        for k in range(2):
            who = 2 * there + (c if k == 0 else 1 - c)
            lhs[:, pl.ds(pl.multiple_of(who * 256, 256), 256)] = chunk_refs[2 * j + k][...]
    total = res_ref[...].astype(F32) + jnp.dot(
        lhs[...], w_ref[...], preferred_element_type=F32
    )
    half = a_ref.shape[0]
    a_ref[...] = total[0:half].astype(BF16)
    b_ref[...] = total[half:].astype(BF16)


def normed_body(pos_ref, *refs):
    ins, gain_ref, out_ref = refs[:8], refs[8], refs[9]
    size = ins[0].shape[0]
    for k in range(2):
        full = [r[...].astype(F32) for r in ins[4 * k : 4 * k + 4]]
        square = sum(jnp.sum(v * v, axis=1, keepdims=True) for v in full)
        scale = lax.rsqrt(square * (1.0 / 2048.0) + EPSILON)
        for v, shift in zip(full, SHIFTS):
            at = lax.rem(pos_ref[0] + shift + 4, 4)
            lanes = pl.ds(pl.multiple_of(at * 512, 512), 512)
            out_ref[k * size : (k + 1) * size, lanes] = (v * scale * gain_ref[0:1, lanes]).astype(
                BF16
            )


def hidden_chunk(normed, wide_ref, hidden, lanes, width):
    depth = wide_ref.shape[1] * wide_ref.shape[2]
    gate, up = (
        jnp.dot(
            normed[...], wide_ref[part, :, :, lanes].reshape(depth, width),
            preferred_element_type=F32,
        )
        for part in range(2)
    )
    hidden[:, lanes] = (silu(gate) * up).astype(BF16)


def down_part(hidden, down, at, out_a, out_b):
    tall = down.shape[0] // 4
    rows = down[pl.ds(at * tall, tall), :, :].reshape(tall * down.shape[1], down.shape[2])
    contract = (((1,), (1,)), ((), ()))
    part = lax.dot_general(hidden[...], rows, contract, preferred_element_type=F32).astype(BF16)
    half = part.shape[0] // 2
    out_a[...] = part[0:half]
    out_b[...] = part[half:]


SHIFTS = (0, -1, 1, 2)
FAR_FIRST = (3, 1, 2, 0)
AHEAD = 9


def hidden_body(
    pos_ref, normed, w_hbm, far_a, far_b, hidden, down, w_ref, sems, down_sems
):
    x = pos_ref[0]
    width = w_hbm.shape[3] // 3
    groups = w_hbm.shape[0]
    tall = groups // 4
    whole = width // 256
    rest = width - whole * 256
    chunks = 2 * whole
    last = chunks * 256
    starts = [lax.rem(x + s + 4, 4) for s in SHIFTS]

    def pieces(n):
        for part in range(2):
            for k in range(2):
                rows = pl.ds(k * (groups // 2), groups // 2)
                to = w_ref.at[part]
                if n == chunks:
                    for i in range(2):
                        yield pltpu.make_async_copy(
                            w_hbm.at[rows, i, :, part * width + whole * 256 : (part + 1) * width],
                            to.at[rows, :, last + i * rest : last + (i + 1) * rest],
                            sems.at[n, part, 2 * k + i],
                        )
                else:
                    at = part * width + (n % whole) * 256
                    yield pltpu.make_async_copy(
                        w_hbm.at[rows, n // whole, :, at : at + 256],
                        to.at[rows, :, n * 256 : (n + 1) * 256],
                        sems.at[n, part, k],
                    )

    def down_pieces(j):
        rows = pl.ds(starts[j] * tall, tall)
        for i in range(2):
            for k, (lo, hi, to) in enumerate(
                ((0, whole * 256, i * whole * 256), (whole * 256, width, last + i * rest))
            ):
                yield pltpu.make_async_copy(
                    w_hbm.at[rows, i, :, 2 * width + lo : 2 * width + hi],
                    down.at[rows, :, to : to + hi - lo],
                    down_sems.at[j, i, k],
                )

    def begin(copies):
        for each in copies:
            each.start()

    def finish(copies):
        for each in copies:
            each.wait()

    order = [pieces(n) for n in range(chunks + 1)]
    order = [list(each) for each in order] + [list(down_pieces(j)) for j in FAR_FIRST]
    for each in order[:AHEAD]:
        begin(each)
    for n in range(chunks + 1):
        finish(order[n])
        if n + AHEAD < len(order):
            begin(order[n + AHEAD])
        wide = 256 if n < chunks else 2 * rest
        hidden_chunk(normed, w_ref, hidden, slice(n * 256, n * 256 + wide), wide)
    for each in order[chunks + 1 + AHEAD :]:
        begin(each)
    finish(down_pieces(FAR_FIRST[0]))
    down_part(hidden, down, starts[FAR_FIRST[0]], far_a, far_b)
    for j in FAR_FIRST[1:]:
        finish(down_pieces(j))


def near_body(pos_ref, hidden, down, *outs):
    for k, j in enumerate(FAR_FIRST[1:]):
        at = lax.rem(pos_ref[0] + SHIFTS[j] + 4, 4)
        down_part(hidden, down, at, outs[2 * k], outs[2 * k + 1])


def last_body(
    pos_ref, sa_ref, pa_ref, la_ref, ra_ref, sb_ref, pb_ref, lb_ref, rb_ref, mine_ref, theirs_ref
):
    c = pos_ref[1]
    size = sa_ref.shape[0]
    parts = ((sa_ref, pa_ref, la_ref, ra_ref), (sb_ref, pb_ref, lb_ref, rb_ref))
    for k, (s_ref, p_ref, left_ref, right_ref) in enumerate(parts):
        at = slice(k * size, (k + 1) * size)
        for ref, who in ((theirs_ref, 1 - c), (mine_ref, c)):
            lanes = pl.ds(pl.multiple_of(who * 256, 256), 256)
            total = (
                p_ref[:, lanes].astype(F32)
                + left_ref[:, lanes].astype(F32)
                + right_ref[:, lanes].astype(F32)
            )
            ref[at, :] = (s_ref[:, lanes].astype(F32) + 0.5 * total).astype(BF16)


def join_body(pos_ref, mine_ref, other_ref, out_ref, sems):
    c = pos_ref[1]
    size = mine_ref.shape[0]
    copies = []
    for k, (half, ref) in enumerate(((c, mine_ref), (1 - c, other_ref))):
        at = pl.ds(pl.multiple_of(half * size, size), size)
        copies.append(pltpu.make_async_copy(ref, out_ref.at[at, :], sems.at[k]))
    for each in copies:
        each.start()
    for each in copies:
        each.wait()


def turned(x, axis, distance):
    n = lax.axis_size(axis)
    return lax.ppermute(x, axis, [(i, (i + distance) % n) for i in range(n)])


def along_x(a, b):
    left_a, right_b = turned(a, "x", 1), turned(b, "x", -1)
    left_b, right_a = turned(b, "x", 1), turned(a, "x", -1)
    far_a, far_b = turned(left_a, "x", 1), turned(right_b, "x", -1)
    return (a, left_a, right_a, far_a), (b, left_b, right_b, far_b)


def shards(
    grouped_head_inputs,
    head_gate_inputs,
    unsmoothed_step,
    head_decay_rate,
    extra_log_decay,
    first_group_keys,
    first_group_queries,
    second_group_keys,
    second_group_queries,
    head_input_filter,
    first_group_filter,
    second_group_filter,
    head_norm_gain,
    output_weight,
    residual,
    channel_norm_gain,
    channel_gate_weight,
    channel_up_weight,
    channel_down_weight,
):
    length = grouped_head_inputs.shape[0]
    half = length // 2
    blocks = length // BLOCK
    xi = lax.axis_index("x").astype(jnp.int32)
    ci = lax.axis_index("c").astype(jnp.int32)
    yi = lax.axis_index("y").astype(jnp.int32)
    zi = lax.axis_index("z").astype(jnp.int32)
    pos = jnp.stack([xi, ci, zi, yi])

    def call(body, outs, args, name, scratch=(), spaces=None, limit=12, flops=None, loose=(), spilled=()):
        spaces = spaces or [pltpu.VMEM] * len(args)
        single = not isinstance(outs, tuple)
        outs = (outs,) if single else outs
        args = [
            a
            if s is pltpu.SMEM
            else pltpu.with_memory_space_constraint(a, pltpu.HBM if i in loose else s)
            for i, (a, s) in enumerate(zip(args, spaces))
        ]
        done = pl.pallas_call(
            body,
            out_shape=tuple(
                (pltpu.HBM if i in spilled else pltpu.VMEM)(o.shape, o.dtype)
                for i, o in enumerate(outs)
            ),
            in_specs=[pl.BlockSpec(memory_space=s) for s in spaces],
            out_specs=tuple(
                pl.BlockSpec(memory_space=pltpu.HBM if name == "join" else pltpu.VMEM)
                for _ in outs
            ),
            scratch_shapes=list(scratch),
            cost_estimate=flops
            and pl.CostEstimate(flops=flops, transcendentals=0, bytes_accessed=10**6),
            compiler_params=pltpu.CompilerParams(vmem_limit_bytes=limit * 2**20),
        )(*args)
        return done[0] if single else done

    def scalar_first(args):
        return [pltpu.SMEM] + [pltpu.VMEM] * (len(args) - 1)

    own_rows = jnp.concatenate(
        [channel_gate_weight, channel_up_weight, channel_down_weight], axis=1
    )
    all_w = lax.all_gather(own_rows, SP + ("c",), axis=0, tiled=True)
    x_flat = grouped_head_inputs.reshape(length, 256)
    k2t, q2t = second_group_keys.T, second_group_queries.T
    packed = pack_rim(x_flat, first_group_keys, first_group_queries, k2t, q2t)
    count = lax.axis_size(SP)
    rim = lax.ppermute(packed, SP, [(i, i + 1) for i in range(count - 1)])

    args = (
        head_decay_rate, x_flat, first_group_keys, first_group_queries, k2t, q2t, rim,
        head_input_filter, first_group_filter, second_group_filter,
        unsmoothed_step.transpose(1, 2, 0), extra_log_decay.transpose(1, 2, 0),
    )
    xc, k1c, q1c, kq2c, cum, soft, s1, s2, lead, end = call(
        states_body,
        (
            shape((length, 256), BF16),
            shape((length, 128), BF16),
            shape((length, 128), BF16),
            shape((length, 128), BF16),
            shape((8 * blocks, BLOCK), F32),
            shape((8 * blocks, BLOCK), F32),
            shape((length, 128), BF16),
            shape((length, 128), BF16),
            shape((8 * blocks, 128), F32),
            shape((208, 128), BF16),
        ),
        args,
        "states",
        loose=(1, 2, 3, 4, 5, 7, 8, 9, 10, 11),
        spilled=(1, 6, 7),
        scratch=(
            pltpu.VMEM((length + 8, 640), F32),
            pltpu.VMEM((8, 640), F32),
            pltpu.VMEM((8 * blocks, BLOCK), F32),
            pltpu.VMEM((8 * blocks, BLOCK), F32),
        ),
        spaces=scalar_first(args),
    )
    output_weight, residual, head_gate_inputs, end = lax.optimization_barrier(
        (output_weight, residual, head_gate_inputs, end)
    )
    before = [turned(end, "y", k) for k in (1, 2, 3)]
    args = (pos, end, *before)
    pre, ylead, total = call(
        combine_body,
        (shape((192, 128), F32), shape((8, 128), F32), shape((lax.axis_size("z"), 208, 128), BF16)),
        args,
        "combine",
        spaces=scalar_first(args),
    )
    rows = lax.all_to_all(total, "z", 0, 0, tiled=True)
    xc = lax.optimization_barrier((xc, total))[0]
    inside = call(
        inside_body,
        shape((length, 256), F32),
        (xc, k1c, q1c, kq2c, cum, soft),
        "inside",
        loose=(1,),
    )
    gates = head_gate_inputs.reshape(length, 256)
    args = (
        pos, inside, gates, q1c, kq2c, cum, s1, s2, lead, head_norm_gain, pre, ylead, rows
    )
    mine, theirs = call(
        mixed_body,
        (shape((half, 256), BF16), shape((half, 256), BF16)),
        args,
        "mixed",
        loose=(2, 6, 7, 9),
        spaces=scalar_first(args),
    )
    other = turned(theirs, "c", 1)

    w = output_weight.reshape(2, 8, 128, 256).transpose(1, 0, 2, 3).reshape(2048, 256)
    w_other = turned(w, "c", 1)
    res_other = turned(lax.dynamic_slice_in_dim(residual, (1 - ci) * half, half, axis=0), "c", 1)
    w_both = jnp.where(
        ci == 0, jnp.concatenate([w, w_other], 1), jnp.concatenate([w_other, w], 1)
    )
    res_mine = lax.dynamic_slice_in_dim(residual, ci * half, half, axis=0)
    res_both = jnp.where(
        ci == 0,
        jnp.concatenate([res_mine, res_other], 1),
        jnp.concatenate([res_other, res_mine], 1),
    )

    ours, others = along_x(mine, other)
    args = (pos, *(v for pair in zip(ours, others) for v in pair), w_both, res_both)
    stream_a, stream_b = call(
        projection_body,
        (shape((half // 2, 512), BF16), shape((half // 2, 512), BF16)),
        args,
        "projection",
        scratch=(pltpu.VMEM((half, 2048), BF16),),
        spaces=scalar_first(args),
    )
    all_a, all_b = along_x(stream_a, stream_b)
    quarter = shape((half // 2, 512), BF16)
    shard_rows, shard_cols = own_rows.shape
    all_w = all_w.reshape(-1, 2, shard_rows, shard_cols)
    wide = (all_w.shape[0], shard_rows, shard_cols // 3 * 2)

    normed = call(
        normed_body,
        shape((half, 2048), BF16),
        (pos, *all_a, *all_b, channel_norm_gain[None]),
        "normed",
        loose=(9,),
        spaces=[pltpu.SMEM] + [pltpu.VMEM] * 9,
    )
    pa3, pb3, hidden, down = call(
        hidden_body,
        (quarter, quarter, shape((half, wide[2]), BF16), shape(wide, BF16)),
        (pos, normed, all_w),
        "hidden",
        scratch=(
            pltpu.VMEM((2, *wide), BF16),
            pltpu.SemaphoreType.DMA((shard_cols // 3 // 256 * 2 + 1, 2, 4)),
            pltpu.SemaphoreType.DMA((4, 2, 2)),
        ),
        spaces=[pltpu.SMEM, pltpu.VMEM, pltpu.HBM],
        limit=20,
    )
    far_a = turned(pa3, "x", 1)
    far_b = turned(pb3, "x", -1)
    pa1, pb1, pa2, pb2, pa0, pb0 = call(
        near_body,
        (quarter,) * 6,
        (pos, hidden, down),
        "near",
        spaces=[pltpu.SMEM] + [pltpu.VMEM] * 2,
    )
    left_b = turned(pb2, "x", 1)
    right_a = turned(pa1, "x", -1)
    sum_a = (pa2.astype(F32) + far_a.astype(F32)).astype(BF16)
    left_a = turned(sum_a, "x", 1)
    sum_b = (pb1.astype(F32) + far_b.astype(F32)).astype(BF16)
    right_b = turned(sum_b, "x", -1)
    mine, theirs = call(
        last_body,
        (shape((half, 256), BF16),) * 2,
        (pos, stream_a, pa0, left_a, right_a, stream_b, pb0, left_b, right_b),
        "last",
        spaces=[pltpu.SMEM] + [pltpu.VMEM] * 8,
    )
    other = turned(theirs, "c", 1)
    return call(
        join_body,
        shape((length, 256), BF16),
        (pos, mine, other),
        "join",
        spilled=(0,),
        scratch=(pltpu.SemaphoreType.DMA((2,)),),
        spaces=[pltpu.SMEM] + [pltpu.VMEM] * 2,
    )


def solution(mesh):
    sp, tp = mesh.devices.shape
    wide = Mesh(mesh.devices.reshape(sp // 4, 4, tp // 2, 2), ("z", "y", "x", "c"))

    return jax.shard_map(
        shards,
        mesh=wide,
        in_specs=(
            P(SP, None, TP),
            P(SP, None, TP),
            P(SP, None, TP),
            P(None, TP),
            P(SP, None, TP),
            P(SP, None),
            P(SP, None),
            P(SP, None),
            P(SP, None),
            P(None, None, TP),
            P(),
            P(),
            P(None, TP),
            P(None, None, TP),
            P(SP, TP),
            P(),
            P(SP, TP),
            P(SP, TP),
            P(SP, TP),
        ),
        out_specs=P(SP, TP),
        check_vma=False,
    )
```

profile of v0, /device:TPU:1, one launch (start us, length us, event | category | flops | bytes accessed | tf_op | source)
XLA Modules:
  0.0 155.9 jit_solution(12809244938700076503)
XLA Ops:
  6.5 1.7 %pad_maximum_fusion = bf16[64,1920]{1,0:T(8,128)(2,1)} fusion(bf16[64,640]{1,0:T(8,128)(2,1)} %param.37, bf16[64,640]{1,0:T(8,128)(2,1)} %param.36, bf16[64,640]{1,0:T(8,128)(2,1)} %param.35), kind=kLoop, calls=%fused_computation.6 | loop fusion | flops 737280 | bytes 491520 | tf_op jit(solution)/shard_map/concatenate | solution.py:583
  8.3 1.9 %copy.26 = bf16[128,8,2,128]{3,1,2,0:T(8,128)(2,1)} copy(bf16[128,8,2,128]{3,2,1,0:T(2,128)(2,1)} %bitcast.27) | data formatting | bytes 1048576
  10.2 1.6 %pack_rim.1 = bf16[16,640]{1,0:T(8,128)(2,1)} custom-call(bf16[1024,256]{1,0:T(8,128)(2,1)} %bitcast.23, bf16[1024,128]{1,0:T(8,128)(2,1)} %k1_ref.3, bf16[1024,128]{1,0:T(8,128)(2,1)} %q1_ref.3, bf16[64,1024]{1,0:T(8,128)(2,1)} %bitcast.29, bf16[64,1024]{1,0:T(8,128)(2,1)} %bitcast.31), custom_call_target="tpu_custom_call" | custom-call | tf_op jit(solution)/shard_map/pack_rim/pallas_call | solution.py:36
  11.8 4.0 %collective-permute-start = (bf16[16,640]{1,0:T(8,128)(2,1)}, bf16[16,640]{1,0:T(8,128)(2,1)S(1)}, u32[]{:S(2)}, u32[]{:S(2)}) collective-permute-start(bf16[16,640]{1,0:T(8,128)(2,1)} %pack_rim.1), channel_id=1, source_target_pairs={{0,8},{8,16},{16,24},{24,32},{32,40},{40,48},{48,56},{56,64},{64,7... | collective-permute-start | bytes 61448 | tf_op jit(solution)/shard_map/ppermute | solution.py:591
  16.9 7.0 %shard_map.181 = (bf16[1024,256]{1,0:T(8,128)(2,1)S(1)}, bf16[1024,128]{1,0:T(8,128)(2,1)}, bf16[1024,128]{1,0:T(8,128)(2,1)S(1)}, bf16[1024,128]{1,0:T(8,128)(2...) custom-call(f32[2,2]{1,0:T(2,128)S(1)} %copy-done, ...), custom_call_target="tpu_custom_call" | custom-call | tf_op jit(solution)/shard_map/pallas_call | solution.py:562
  23.9 3.2 %collective-permute-start.3 = (bf16[208,128]{1,0:T(8,128)(2,1)S(1)}, bf16[208,128]{1,0:T(8,128)(2,1)S(1)}, u32[]{:S(2)}, u32[]{:S(2)}) collective-permute-start(bf16[208,128]{1,0:T(8,128)(2,1)S(1)} %get-tuple-element.41.own_ref), channel_id=1, source_target_pairs={{0,24},{8,0},{16,8},{24,16},{1,25},{9,1},{17,9},{25,17},{2,26},{10... | collective-permute-start | bytes 159752 | tf_op jit(solution)/shard_map/ppermute | solution.py:512
  28.5 4.0 %collective-permute-done.2.b2_ref = bf16[208,128]{1,0:T(8,128)(2,1)S(1)} collective-permute-done((bf16[208,128]{1,0:T(8,128)(2,1)S(1)}, bf16[208,128]{1,0:T(8,128)(2,1)S(1)}, u32[]{:S(2)}, u32[]{:S(2)}) %collective-permute-start.2) | collective-permute-done | bytes 53280 | tf_op jit(solution)/shard_map/ppermute | solution.py:512
  34.7 8.9 %all-to-all-start = ((bf16[8,208,128]{2,1,0:T(8,128)(2,1)}), bf16[8,208,128]{2,1,0:T(8,128)(2,1)S(1)}, u32[]{:S(2)}, u32[]{:S(2)}) async-start(bf16[8,208,128]{2,1,0:T(8,128)(2,1)} %get-tuple-element.42), calls=%async_computation | async-start | bytes 851968 | tf_op jit(solution)/shard_map/all_to_all | solution.py:636
  44.7 2.5 %collective-permute-start.11 = (bf16[2048,256]{1,0:T(8,128)(2,1)}, bf16[2048,256]{1,0:T(8,128)(2,1)}, u32[]{:S(2)}, u32[]{:S(2)}) collective-permute-start(bf16[2048,256]{1,0:T(8,128)(2,1)} %bitcast.10), channel_id=1, source_target_pairs={{0,1},{1,0},{2,3},{3,2},{4,5},{5,4},{6,7},{7,6},{8,9},{9,8},{10,11... | collective-permute-start | bytes 3145736 | tf_op jit(solution)/shard_map/ppermute | solution.py:512
  48.0 4.6 %shard_map.183.in_ref = f32[1024,256]{1,0:T(8,128)S(1)} custom-call(bf16[1024,256]{1,0:T(8,128)(2,1)S(1)} %get-tuple-element.43.xc_ref, bf16[1024,128]{1,0:T(8,128)(2,1)} %get-tuple-element.44.k1_ref, bf16[1024,128]{1,0:T(8,128)(2,1)S(1)} %get-tuple-element.45.q1_ref, bf16[1024,128]{1,0:T(8,128)(2,1)S(1)} %get-tuple-element.46.kq2_ref, ...), custom_call_target="tpu_custom_call" | custom-call | tf_op jit(solution)/shard_map/pallas_call | solution.py:562
  52.6 5.3 %all-to-all-done.rows_ref = bf16[8,208,128]{2,1,0:T(8,128)(2,1)S(1)} async-done(((bf16[8,208,128]{2,1,0:T(8,128)(2,1)}), bf16[8,208,128]{2,1,0:T(8,128)(2,1)S(1)}, u32[]{:S(2)}, u32[]{:S(2)}) %all-to-all-start) | async-done | bytes 426016 | tf_op jit(solution)/shard_map/all_to_all | solution.py:636
  57.9 4.1 %shard_map.184 = (bf16[512,256]{1,0:T(8,128)(2,1)S(1)}, bf16[512,256]{1,0:T(8,128)(2,1)S(1)}) custom-call(s32[4]{0:T(128)S(1)} %pad_add_fusion.y_ref.pos_ref, f32[1024,256]{1,0:T(8,128)S(1)} %shard_map.183.in_ref, bf16[1024,256]{1,0:T(8,128)(2,1)} %bitcast.25, bf16[1024,128]{1,0:T(8,128)(2,1)S(1)} %get-tuple-element.45.q1_ref, ...), custom_call_target="tpu_custom_call" | custom-call | tf_op jit(solution)/shard_map/pallas_call | solution.py:562
  62.0 3.0 %collective-permute-start.4 = (bf16[512,256]{1,0:T(8,128)(2,1)S(1)}, bf16[512,256]{1,0:T(8,128)(2,1)S(1)}, u32[]{:S(2)}, u32[]{:S(2)}) collective-permute-start(bf16[512,256]{1,0:T(8,128)(2,1)S(1)} %get-tuple-element.56), channel_id=1, source_target_pairs={{0,1},{1,0},{2,3},{3,2},{4,5},{5,4},{6,7},{7,6},{8,9},{9,8},{10,11... | collective-permute-start | bytes 786440 | tf_op jit(solution)/shard_map/ppermute | solution.py:512
  66.4 2.4 %collective-permute-start.8 = (bf16[512,256]{1,0:T(8,128)(2,1)S(1)}, bf16[512,256]{1,0:T(8,128)(2,1)S(1)}, u32[]{:S(2)}, u32[]{:S(2)}) collective-permute-start(bf16[512,256]{1,0:T(8,128)(2,1)S(1)} %collective-permute-done.4.refs_1_), channel_id=1, source_target_pairs={{0,6},{2,0},{4,2},{6,4},{1,7},{3,1},{5,3},{7,5},{8,14},{10,8},{12,... | collective-permute-start | bytes 786440 | tf_op jit(solution)/shard_map/ppermute | solution.py:512
  70.4 3.6 %collective-permute-done.5.refs_2_ = bf16[512,256]{1,0:T(8,128)(2,1)S(1)} collective-permute-done((bf16[512,256]{1,0:T(8,128)(2,1)S(1)}, bf16[512,256]{1,0:T(8,128)(2,1)S(1)}, u32[]{:S(2)}, u32[]{:S(2)}) %collective-permute-start.5) | collective-permute-done | bytes 262176 | tf_op jit(solution)/shard_map/ppermute | solution.py:512
  74.0 3.5 %collective-permute-start.10 = (bf16[512,256]{1,0:T(8,128)(2,1)S(1)}, bf16[512,256]{1,0:T(8,128)(2,1)S(1)}, u32[]{:S(2)}, u32[]{:S(2)}) collective-permute-start(bf16[512,256]{1,0:T(8,128)(2,1)S(1)} %collective-permute-done.8.refs_5_), channel_id=1, source_target_pairs={{0,6},{2,0},{4,2},{6,4},{1,7},{3,1},{5,3},{7,5},{8,14},{10,8},{12,... | collective-permute-start | bytes 786440 | tf_op jit(solution)/shard_map/ppermute | solution.py:512
  77.5 3.0 %maximum_select_fusion.refs_8_ = bf16[2048,512]{1,0:T(8,128)(2,1)S(1)} fusion(bf16[2048,256]{1,0:T(8,128)(2,1)} %collective-permute-done.11, bf16[2048,256]{1,0:T(8,128)(2,1)} %bitcast.10, pred[]{:T(512)S(6)} %eq.4), kind=kLoop, calls=%fused_computation | loop fusion | flops 9437184 | bytes 4194305 | tf_op jit(solution)/shard_map/jit(_where)/select_n | solution.py:662
  80.5 4.7 %collective-permute-done.9.refs_6_ = bf16[512,256]{1,0:T(8,128)(2,1)S(1)} collective-permute-done((bf16[512,256]{1,0:T(8,128)(2,1)S(1)}, bf16[512,256]{1,0:T(8,128)(2,1)S(1)}, u32[]{:S(2)}, u32[]{:S(2)}) %collective-permute-start.9) | collective-permute-done | bytes 262176 | tf_op jit(solution)/shard_map/ppermute | solution.py:512
  85.3 2.1 %shard_map.185 = (bf16[256,512]{1,0:T(8,128)(2,1)S(1)}, bf16[256,512]{1,0:T(8,128)(2,1)S(1)}) custom-call(s32[4]{0:T(128)S(1)} %pad_add_fusion.y_ref.pos_ref, bf16[512,256]{1,0:T(8,128)(2,1)S(1)} %get-tuple-element.55.refs_0_, bf16[512,256]{1,0:T(8,128)(2,1)S(1)} %collective-permute-done.4.refs_1_, bf16[512,256]{1,0:T(8,128)(2,1)S(1)} %collective-permute-done.5.refs_2_, ...), custom_call_target="tpu_custom_call" | custom-call | tf_op jit(solution)/shard_map/pallas_call | solution.py:562
  88.3 2.7 %collective-permute-start.17 = (bf16[256,512]{1,0:T(8,128)(2,1)S(1)}, bf16[256,512]{1,0:T(8,128)(2,1)S(1)}, u32[]{:S(2)}, u32[]{:S(2)}) collective-permute-start(bf16[256,512]{1,0:T(8,128)(2,1)S(1)} %get-tuple-element.60.refs_4_.sb_ref), channel_id=1, source_target_pairs={{0,6},{2,0},{4,2},{6,4},{1,7},{3,1},{5,3},{7,5},{8,14},{10,8},{12,... | collective-permute-start | bytes 786440 | tf_op jit(solution)/shard_map/ppermute | solution.py:512
  92.5 4.1 %collective-permute-done.13.refs_1_ = bf16[256,512]{1,0:T(8,128)(2,1)S(1)} collective-permute-done((bf16[256,512]{1,0:T(8,128)(2,1)S(1)}, bf16[256,512]{1,0:T(8,128)(2,1)S(1)}, u32[]{:S(2)}, u32[]{:S(2)}) %collective-permute-start.13) | collective-permute-done | bytes 262176 | tf_op jit(solution)/shard_map/ppermute | solution.py:512
  96.6 2.7 %collective-permute-start.18 = (bf16[256,512]{1,0:T(8,128)(2,1)S(1)}, bf16[256,512]{1,0:T(8,128)(2,1)S(1)}, u32[]{:S(2)}, u32[]{:S(2)}) collective-permute-start(bf16[256,512]{1,0:T(8,128)(2,1)S(1)} %collective-permute-done.17.refs_6_), channel_id=1, source_target_pairs={{0,6},{2,0},{4,2},{6,4},{1,7},{3,1},{5,3},{7,5},{8,14},{10,8},{12,... | collective-permute-start | bytes 786440 | tf_op jit(solution)/shard_map/ppermute | solution.py:512
  99.3 1.9 %collective-permute-done.14.refs_2_ = bf16[256,512]{1,0:T(8,128)(2,1)S(1)} collective-permute-done((bf16[256,512]{1,0:T(8,128)(2,1)S(1)}, bf16[256,512]{1,0:T(8,128)(2,1)S(1)}, u32[]{:S(2)}, u32[]{:S(2)}) %collective-permute-start.14) | collective-permute-done | bytes 262176 | tf_op jit(solution)/shard_map/ppermute | solution.py:512
  102.2 5.6 %collective-permute-done.15.refs_3_ = bf16[256,512]{1,0:T(8,128)(2,1)S(1)} collective-permute-done((bf16[256,512]{1,0:T(8,128)(2,1)S(1)}, bf16[256,512]{1,0:T(8,128)(2,1)S(1)}, u32[]{:S(2)}, u32[]{:S(2)}) %collective-permute-start.15) | collective-permute-done | bytes 262176 | tf_op jit(solution)/shard_map/ppermute | solution.py:512
  109.3 3.8 %all-gather.2.cloned.1.call-done = bf16[4096,1920]{1,0:T(8,128)(2,1)} async-done(((bf16[64,1920]{1,0:T(8,128)(2,1)}), bf16[4096,1920]{1,0:T(8,128)(2,1)}) %all-gather.2.cloned.1.call-update) | async-done | bytes 15728656 | tf_op jit(solution)/shard_map/all_gather | solution.py:586
  113.1 9.9 %shard_map.187 = (bf16[256,512]{1,0:T(8,128)(2,1)S(1)}, bf16[256,512]{1,0:T(8,128)(2,1)S(1)}, bf16[512,1280]{1,0:T(8,128)(2,1)S(1)}, bf16[32,64,1280]{2,1,0:T(8,128)(2,1)S(1)}) custom-call(s32[4]{0:T(128)S(1)} %pad_add_fusion.y_ref.pos_ref, bf16[512,2048]{1,0:T(8,128)(2,1)S(1)} %shard_map.186.normed, bf16[32,2,64,1920]{3,2,1,0:T(8,128)(2,1)} %bitcast.22), custom_call_target="tpu_custom_call" | custom-call | tf_op jit(solution)/shard_map/pallas_call | solution.py:562
  126.0 2.8 %shard_map.188 = (bf16[256,512]{1,0:T(8,128)(2,1)S(1)}, bf16[256,512]{1,0:T(8,128)(2,1)S(1)}, bf16[256,512]{1,0:T(8,128)(2,1)S(1)}, bf16[256,512]{1,0:T(8,128)(2...) custom-call(s32[4]{0:T(128)S(1)} %pad_add_fusion.y_ref.pos_ref, ...), custom_call_target="tpu_custom_call" | custom-call | tf_op jit(solution)/shard_map/pallas_call | solution.py:562
  130.3 1.8 %collective-permute-done.19 = bf16[256,512]{1,0:T(8,128)(2,1)S(1)} collective-permute-done((bf16[256,512]{1,0:T(8,128)(2,1)S(1)}, bf16[256,512]{1,0:T(8,128)(2,1)S(1)}, u32[]{:S(2)}, u32[]{:S(2)}) %collective-permute-start.19) | collective-permute-done | bytes 262176 | tf_op jit(solution)/shard_map/ppermute | solution.py:512
  132.4 2.7 %collective-permute-start.24 = (bf16[256,512]{1,0:T(8,128)(2,1)S(1)}, bf16[256,512]{1,0:T(8,128)(2,1)S(1)}, u32[]{:S(2)}, u32[]{:S(2)}) collective-permute-start(bf16[256,512]{1,0:T(8,128)(2,1)S(1)} %add_convert_fusion), channel_id=1, source_target_pairs={{0,6},{2,0},{4,2},{6,4},{1,7},{3,1},{5,3},{7,5},{8,14},{10,8},{12,... | collective-permute-start | bytes 786440 | tf_op jit(solution)/shard_map/ppermute | solution.py:512
  135.1 2.3 %collective-permute-done.21.ra_ref = bf16[256,512]{1,0:T(8,128)(2,1)S(1)} collective-permute-done((bf16[256,512]{1,0:T(8,128)(2,1)S(1)}, bf16[256,512]{1,0:T(8,128)(2,1)S(1)}, u32[]{:S(2)}, u32[]{:S(2)}) %collective-permute-start.21) | collective-permute-done | bytes 262176 | tf_op jit(solution)/shard_map/ppermute | solution.py:512
  138.0 5.6 %collective-permute-done.20.la_ref = bf16[256,512]{1,0:T(8,128)(2,1)S(1)} collective-permute-done((bf16[256,512]{1,0:T(8,128)(2,1)S(1)}, bf16[256,512]{1,0:T(8,128)(2,1)S(1)}, u32[]{:S(2)}, u32[]{:S(2)}) %collective-permute-start.20) | collective-permute-done | bytes 262176 | tf_op jit(solution)/shard_map/ppermute | solution.py:512
  144.5 2.0 %collective-permute-start.25 = (bf16[512,256]{1,0:T(8,128)(2,1)S(1)}, bf16[512,256]{1,0:T(8,128)(2,1)S(1)}, u32[]{:S(2)}, u32[]{:S(2)}) collective-permute-start(bf16[512,256]{1,0:T(8,128)(2,1)S(1)} %get-tuple-element.72), channel_id=1, source_target_pairs={{0,1},{1,0},{2,3},{3,2},{4,5},{5,4},{6,7},{7,6},{8,9},{9,8},{10,11... | collective-permute-start | bytes 786440 | tf_op jit(solution)/shard_map/ppermute | solution.py:512
  (54 shorter events, 23.5 us)
Async XLA Ops:
  6.5 10.4 %copy-start = (f32[2,2]{1,0:T(2,128)S(1)}, f32[2,2]{1,0:T(2,128)}, u32[]{:S(2)}) copy-start(f32[2,2]{1,0:T(2,128)} %rate_ref.1) | copy-start | bytes 52
  6.5 106.6 %all-gather.2.cloned.1.call-start = ((), (), s32[]{:S(2)}) async-start(), calls=%async_computation.1 | async-start | bytes 15974400 | tf_op jit(solution)/shard_map/all_gather | solution.py:586
  10.2 33.4 %copy-start.1 = (bf16[2,1024,256]{2,1,0:T(8,128)(2,1)S(1)}, bf16[2,1024,256]{2,1,0:T(8,128)(2,1)}, u32[]{:S(2)}) copy-start(bf16[2,1024,256]{2,1,0:T(8,128)(2,1)} %param.32) | copy-start | bytes 3145732
  11.8 5.1 %collective-permute-start = (bf16[16,640]{1,0:T(8,128)(2,1)}, bf16[16,640]{1,0:T(8,128)(2,1)S(1)}, u32[]{:S(2)}, u32[]{:S(2)}) collective-permute-start(bf16[16,640]{1,0:T(8,128)(2,1)} %pack_rim.1), channel_id=1, source_target_pairs={{0,8},{8,16},{16,24},{24,32},{32,40},{40,48},{48,56},{56,64},{64,7... | collective-permute-start | bytes 61448 | tf_op jit(solution)/shard_map/ppermute | solution.py:591
  16.9 30.3 %copy-start.3 = (bf16[1024,2,128]{2,1,0:T(2,128)(2,1)S(1)}, bf16[1024,2,128]{2,1,0:T(2,128)(2,1)}, u32[]{:S(2)}) copy-start(bf16[1024,2,128]{2,1,0:T(2,128)(2,1)} %param.20) | copy-start | bytes 1572868
  23.9 4.6 %collective-permute-start.3 = (bf16[208,128]{1,0:T(8,128)(2,1)S(1)}, bf16[208,128]{1,0:T(8,128)(2,1)S(1)}, u32[]{:S(2)}, u32[]{:S(2)}) collective-permute-start(bf16[208,128]{1,0:T(8,128)(2,1)S(1)} %get-tuple-element.41.own_ref), channel_id=1, source_target_pairs={{0,24},{8,0},{16,8},{24,16},{1,25},{9,1},{17,9},{25,17},{2,26},{10... | collective-permute-start | bytes 159752 | tf_op jit(solution)/shard_map/ppermute | solution.py:512
  27.0 5.5 %collective-permute-start.2 = (bf16[208,128]{1,0:T(8,128)(2,1)S(1)}, bf16[208,128]{1,0:T(8,128)(2,1)S(1)}, u32[]{:S(2)}, u32[]{:S(2)}) collective-permute-start(bf16[208,128]{1,0:T(8,128)(2,1)S(1)} %get-tuple-element.41.own_ref), channel_id=1, source_target_pairs={{0,16},{8,24},{16,0},{24,8},{1,17},{9,25},{17,1},{25,9},{2,18},{10... | collective-permute-start | bytes 159752 | tf_op jit(solution)/shard_map/ppermute | solution.py:512
  27.4 6.0 %collective-permute-start.1 = (bf16[208,128]{1,0:T(8,128)(2,1)S(1)}, bf16[208,128]{1,0:T(8,128)(2,1)S(1)}, u32[]{:S(2)}, u32[]{:S(2)}) collective-permute-start(bf16[208,128]{1,0:T(8,128)(2,1)S(1)} %get-tuple-element.41.own_ref), channel_id=1, source_target_pairs={{0,8},{8,16},{16,24},{24,0},{1,9},{9,17},{17,25},{25,1},{2,10},{10... | collective-permute-start | bytes 159752 | tf_op jit(solution)/shard_map/ppermute | solution.py:512
  34.7 23.2 %all-to-all-start = ((bf16[8,208,128]{2,1,0:T(8,128)(2,1)}), bf16[8,208,128]{2,1,0:T(8,128)(2,1)S(1)}, u32[]{:S(2)}, u32[]{:S(2)}) async-start(bf16[8,208,128]{2,1,0:T(8,128)(2,1)} %get-tuple-element.42), calls=%async_computation | async-start | bytes 851968 | tf_op jit(solution)/shard_map/all_to_all | solution.py:636
  44.7 32.9 %collective-permute-start.11 = (bf16[2048,256]{1,0:T(8,128)(2,1)}, bf16[2048,256]{1,0:T(8,128)(2,1)}, u32[]{:S(2)}, u32[]{:S(2)}) collective-permute-start(bf16[2048,256]{1,0:T(8,128)(2,1)} %bitcast.10), channel_id=1, source_target_pairs={{0,1},{1,0},{2,3},{3,2},{4,5},{5,4},{6,7},{7,6},{8,9},{9,8},{10,11... | collective-permute-start | bytes 3145736 | tf_op jit(solution)/shard_map/ppermute | solution.py:512
  52.6 12.4 %copy-start.2 = (bf16[1024,256]{1,0:T(8,128)(2,1)S(1)}, bf16[1024,256]{1,0:T(8,128)(2,1)}, u32[]{:S(2)}) copy-start(bf16[1024,256]{1,0:T(8,128)(2,1)} %param.33) | copy-start | bytes 1572868
  62.0 4.4 %collective-permute-start.4 = (bf16[512,256]{1,0:T(8,128)(2,1)S(1)}, bf16[512,256]{1,0:T(8,128)(2,1)S(1)}, u32[]{:S(2)}, u32[]{:S(2)}) collective-permute-start(bf16[512,256]{1,0:T(8,128)(2,1)S(1)} %get-tuple-element.56), channel_id=1, source_target_pairs={{0,1},{1,0},{2,3},{3,2},{4,5},{5,4},{6,7},{7,6},{8,9},{9,8},{10,11... | collective-permute-start | bytes 786440 | tf_op jit(solution)/shard_map/ppermute | solution.py:512
  65.0 3.7 %collective-permute-start.12 = (bf16[512,256]{1,0:T(8,128)(2,1)S(1)}, bf16[512,256]{1,0:T(8,128)(2,1)S(1)}, u32[]{:S(2)}, u32[]{:S(2)}) collective-permute-start(bf16[512,256]{1,0:T(8,128)(2,1)S(1)} %get-tuple-element.74), channel_id=1, source_target_pairs={{0,1},{1,0},{2,3},{3,2},{4,5},{5,4},{6,7},{7,6},{8,9},{9,8},{10,11... | collective-permute-start | bytes 786440 | tf_op jit(solution)/shard_map/ppermute | solution.py:512
  65.2 8.8 %collective-permute-start.5 = (bf16[512,256]{1,0:T(8,128)(2,1)S(1)}, bf16[512,256]{1,0:T(8,128)(2,1)S(1)}, u32[]{:S(2)}, u32[]{:S(2)}) collective-permute-start(bf16[512,256]{1,0:T(8,128)(2,1)S(1)} %get-tuple-element.55.refs_0_), channel_id=1, source_target_pairs={{0,2},{2,4},{4,6},{6,0},{1,3},{3,5},{5,7},{7,1},{8,10},{10,12},{12... | collective-permute-start | bytes 786440 | tf_op jit(solution)/shard_map/ppermute | solution.py:512
  66.4 7.7 %collective-permute-start.8 = (bf16[512,256]{1,0:T(8,128)(2,1)S(1)}, bf16[512,256]{1,0:T(8,128)(2,1)S(1)}, u32[]{:S(2)}, u32[]{:S(2)}) collective-permute-start(bf16[512,256]{1,0:T(8,128)(2,1)S(1)} %collective-permute-done.4.refs_1_), channel_id=1, source_target_pairs={{0,6},{2,0},{4,2},{6,4},{1,7},{3,1},{5,3},{7,5},{8,14},{10,8},{12,... | collective-permute-start | bytes 786440 | tf_op jit(solution)/shard_map/ppermute | solution.py:512
  68.9 11.6 %collective-permute-start.7 = (bf16[512,256]{1,0:T(8,128)(2,1)S(1)}, bf16[512,256]{1,0:T(8,128)(2,1)S(1)}, u32[]{:S(2)}, u32[]{:S(2)}) collective-permute-start(bf16[512,256]{1,0:T(8,128)(2,1)S(1)} %get-tuple-element.55.refs_0_), channel_id=1, source_target_pairs={{0,6},{2,0},{4,2},{6,4},{1,7},{3,1},{5,3},{7,5},{8,14},{10,8},{12,... | collective-permute-start | bytes 786440 | tf_op jit(solution)/shard_map/ppermute | solution.py:512
  69.5 11.0 %collective-permute-start.6 = (bf16[512,256]{1,0:T(8,128)(2,1)S(1)}, bf16[512,256]{1,0:T(8,128)(2,1)S(1)}, u32[]{:S(2)}, u32[]{:S(2)}) collective-permute-start(bf16[512,256]{1,0:T(8,128)(2,1)S(1)} %collective-permute-done.4.refs_1_), channel_id=1, source_target_pairs={{0,2},{2,4},{4,6},{6,0},{1,3},{3,5},{5,7},{7,1},{8,10},{10,12},{12... | collective-permute-start | bytes 786440 | tf_op jit(solution)/shard_map/ppermute | solution.py:512
  74.0 11.2 %collective-permute-start.9 = (bf16[512,256]{1,0:T(8,128)(2,1)S(1)}, bf16[512,256]{1,0:T(8,128)(2,1)S(1)}, u32[]{:S(2)}, u32[]{:S(2)}) collective-permute-start(bf16[512,256]{1,0:T(8,128)(2,1)S(1)} %collective-permute-done.5.refs_2_), channel_id=1, source_target_pairs={{0,2},{2,4},{4,6},{6,0},{1,3},{3,5},{5,7},{7,1},{8,10},{10,12},{12... | collective-permute-start | bytes 786440 | tf_op jit(solution)/shard_map/ppermute | solution.py:512
  74.0 11.2 %collective-permute-start.10 = (bf16[512,256]{1,0:T(8,128)(2,1)S(1)}, bf16[512,256]{1,0:T(8,128)(2,1)S(1)}, u32[]{:S(2)}, u32[]{:S(2)}) collective-permute-start(bf16[512,256]{1,0:T(8,128)(2,1)S(1)} %collective-permute-done.8.refs_5_), channel_id=1, source_target_pairs={{0,6},{2,0},{4,2},{6,4},{1,7},{3,1},{5,3},{7,5},{8,14},{10,8},{12,... | collective-permute-start | bytes 786440 | tf_op jit(solution)/shard_map/ppermute | solution.py:512
  87.3 9.3 %collective-permute-start.13 = (bf16[256,512]{1,0:T(8,128)(2,1)S(1)}, bf16[256,512]{1,0:T(8,128)(2,1)S(1)}, u32[]{:S(2)}, u32[]{:S(2)}) collective-permute-start(bf16[256,512]{1,0:T(8,128)(2,1)S(1)} %get-tuple-element.59.refs_0_.sa_ref), channel_id=1, source_target_pairs={{0,2},{2,4},{4,6},{6,0},{1,3},{3,5},{5,7},{7,1},{8,10},{10,12},{12... | collective-permute-start | bytes 786440 | tf_op jit(solution)/shard_map/ppermute | solution.py:512
  88.3 8.3 %collective-permute-start.17 = (bf16[256,512]{1,0:T(8,128)(2,1)S(1)}, bf16[256,512]{1,0:T(8,128)(2,1)S(1)}, u32[]{:S(2)}, u32[]{:S(2)}) collective-permute-start(bf16[256,512]{1,0:T(8,128)(2,1)S(1)} %get-tuple-element.60.refs_4_.sb_ref), channel_id=1, source_target_pairs={{0,6},{2,0},{4,2},{6,4},{1,7},{3,1},{5,3},{7,5},{8,14},{10,8},{12,... | collective-permute-start | bytes 786440 | tf_op jit(solution)/shard_map/ppermute | solution.py:512
  91.0 10.2 %collective-permute-start.14 = (bf16[256,512]{1,0:T(8,128)(2,1)S(1)}, bf16[256,512]{1,0:T(8,128)(2,1)S(1)}, u32[]{:S(2)}, u32[]{:S(2)}) collective-permute-start(bf16[256,512]{1,0:T(8,128)(2,1)S(1)} %get-tuple-element.59.refs_0_.sa_ref), channel_id=1, source_target_pairs={{0,6},{2,0},{4,2},{6,4},{1,7},{3,1},{5,3},{7,5},{8,14},{10,8},{12,... | collective-permute-start | bytes 786440 | tf_op jit(solution)/shard_map/ppermute | solution.py:512
  92.4 9.8 %collective-permute-start.16 = (bf16[256,512]{1,0:T(8,128)(2,1)S(1)}, bf16[256,512]{1,0:T(8,128)(2,1)S(1)}, u32[]{:S(2)}, u32[]{:S(2)}) collective-permute-start(bf16[256,512]{1,0:T(8,128)(2,1)S(1)} %get-tuple-element.60.refs_4_.sb_ref), channel_id=1, source_target_pairs={{0,2},{2,4},{4,6},{6,0},{1,3},{3,5},{5,7},{7,1},{8,10},{10,12},{12... | collective-permute-start | bytes 786440 | tf_op jit(solution)/shard_map/ppermute | solution.py:512
  96.6 11.2 %collective-permute-start.15 = (bf16[256,512]{1,0:T(8,128)(2,1)S(1)}, bf16[256,512]{1,0:T(8,128)(2,1)S(1)}, u32[]{:S(2)}, u32[]{:S(2)}) collective-permute-start(bf16[256,512]{1,0:T(8,128)(2,1)S(1)} %collective-permute-done.13.refs_1_), channel_id=1, source_target_pairs={{0,2},{2,4},{4,6},{6,0},{1,3},{3,5},{5,7},{7,1},{8,10},{10,12},{12... | collective-permute-start | bytes 786440 | tf_op jit(solution)/shard_map/ppermute | solution.py:512
  96.6 11.2 %collective-permute-start.18 = (bf16[256,512]{1,0:T(8,128)(2,1)S(1)}, bf16[256,512]{1,0:T(8,128)(2,1)S(1)}, u32[]{:S(2)}, u32[]{:S(2)}) collective-permute-start(bf16[256,512]{1,0:T(8,128)(2,1)S(1)} %collective-permute-done.17.refs_6_), channel_id=1, source_target_pairs={{0,6},{2,0},{4,2},{6,4},{1,7},{3,1},{5,3},{7,5},{8,14},{10,8},{12,... | collective-permute-start | bytes 786440 | tf_op jit(solution)/shard_map/ppermute | solution.py:512
  123.0 9.1 %collective-permute-start.19 = (bf16[256,512]{1,0:T(8,128)(2,1)S(1)}, bf16[256,512]{1,0:T(8,128)(2,1)S(1)}, u32[]{:S(2)}, u32[]{:S(2)}) collective-permute-start(bf16[256,512]{1,0:T(8,128)(2,1)S(1)} %get-tuple-element.65), channel_id=1, source_target_pairs={{0,2},{2,4},{4,6},{6,0},{1,3},{3,5},{5,7},{7,1},{8,10},{10,12},{12... | collective-permute-start | bytes 786440 | tf_op jit(solution)/shard_map/ppermute | solution.py:512
  124.5 7.8 %collective-permute-start.23 = (bf16[256,512]{1,0:T(8,128)(2,1)S(1)}, bf16[256,512]{1,0:T(8,128)(2,1)S(1)}, u32[]{:S(2)}, u32[]{:S(2)}) collective-permute-start(bf16[256,512]{1,0:T(8,128)(2,1)S(1)} %get-tuple-element.70), channel_id=1, source_target_pairs={{0,6},{2,0},{4,2},{6,4},{1,7},{3,1},{5,3},{7,5},{8,14},{10,8},{12,... | collective-permute-start | bytes 786440 | tf_op jit(solution)/shard_map/ppermute | solution.py:512
  128.8 8.7 %collective-permute-start.21 = (bf16[256,512]{1,0:T(8,128)(2,1)S(1)}, bf16[256,512]{1,0:T(8,128)(2,1)S(1)}, u32[]{:S(2)}, u32[]{:S(2)}) collective-permute-start(bf16[256,512]{1,0:T(8,128)(2,1)S(1)} %get-tuple-element.66), channel_id=1, source_target_pairs={{0,6},{2,0},{4,2},{6,4},{1,7},{3,1},{5,3},{7,5},{8,14},{10,8},{12,... | collective-permute-start | bytes 786440 | tf_op jit(solution)/shard_map/ppermute | solution.py:512
  130.1 8.0 %collective-permute-start.22 = (bf16[256,512]{1,0:T(8,128)(2,1)S(1)}, bf16[256,512]{1,0:T(8,128)(2,1)S(1)}, u32[]{:S(2)}, u32[]{:S(2)}) collective-permute-start(bf16[256,512]{1,0:T(8,128)(2,1)S(1)} %get-tuple-element.68), channel_id=1, source_target_pairs={{0,2},{2,4},{4,6},{6,0},{1,3},{3,5},{5,7},{7,1},{8,10},{10,12},{12... | collective-permute-start | bytes 786440 | tf_op jit(solution)/shard_map/ppermute | solution.py:512
  132.2 11.4 %collective-permute-start.20 = (bf16[256,512]{1,0:T(8,128)(2,1)S(1)}, bf16[256,512]{1,0:T(8,128)(2,1)S(1)}, u32[]{:S(2)}, u32[]{:S(2)}) collective-permute-start(bf16[256,512]{1,0:T(8,128)(2,1)S(1)} %add_convert_fusion.1), channel_id=1, source_target_pairs={{0,2},{2,4},{4,6},{6,0},{1,3},{3,5},{5,7},{7,1},{8,10},{10,12},{12... | collective-permute-start | bytes 786440 | tf_op jit(solution)/shard_map/ppermute | solution.py:512
  132.4 11.3 %collective-permute-start.24 = (bf16[256,512]{1,0:T(8,128)(2,1)S(1)}, bf16[256,512]{1,0:T(8,128)(2,1)S(1)}, u32[]{:S(2)}, u32[]{:S(2)}) collective-permute-start(bf16[256,512]{1,0:T(8,128)(2,1)S(1)} %add_convert_fusion), channel_id=1, source_target_pairs={{0,6},{2,0},{4,2},{6,4},{1,7},{3,1},{5,3},{7,5},{8,14},{10,8},{12,... | collective-permute-start | bytes 786440 | tf_op jit(solution)/shard_map/ppermute | solution.py:512
  144.5 3.2 %collective-permute-start.25 = (bf16[512,256]{1,0:T(8,128)(2,1)S(1)}, bf16[512,256]{1,0:T(8,128)(2,1)S(1)}, u32[]{:S(2)}, u32[]{:S(2)}) collective-permute-start(bf16[512,256]{1,0:T(8,128)(2,1)S(1)} %get-tuple-element.72), channel_id=1, source_target_pairs={{0,1},{1,0},{2,3},{3,2},{4,5},{5,4},{6,7},{7,6},{8,9},{9,8},{10,11... | collective-permute-start | bytes 786440 | tf_op jit(solution)/shard_map/ppermute | solution.py:512
Sparse Core Ops, SparseCore 0:
  10.1 103.0 all-gather.1
where the time goes:
time: 156 us
  starting transfers between devices  48.5 us (31%)
  waiting for transfers between devices  47.9 us (31%)
  Pallas kernels  37 us (24%)
  between operations  13.6 us (9%)
  other arithmetic  5.02 us (3%)
  local copies, waits for them, and re-layouts  3.91 us (3%)
    ppermute x25, waiting for transfers between devices, turned(): return lax.ppermute(x, axis, [(i, (i + distance) % n) for i in range(n)])  37.7 us
    ppermute x25, starting transfers between devices, turned(): return lax.ppermute(x, axis, [(i, (i + distance) % n) for i in range(n)])  35.6 us
    pallas_call x10, Pallas kernels, call(): pl.pallas_call(body, out_shape=tuple(((pltpu.HBM if i in spilled else plt...  35.4 us
    all_to_all x1, starting transfers between devices, shards(): rows = lax.all_to_all(total, 'z', 0, 0, tiled=True)  8.9 us
    all_to_all x1, waiting for transfers between devices, shards(): rows = lax.all_to_all(total, 'z', 0, 0, tiled=True)  5.25 us
    ppermute x1, starting transfers between devices, shards(): rim = lax.ppermute(packed, SP, [(i, i + 1) for i in range(count - 1)])  4.01 us
    all_gather x1, waiting for transfers between devices, shards(): all_w = lax.all_gather(own_rows, SP + ('c',), axis=0, tiled=True)  3.82 us
  transfers between devices with their start and end apart: 28, of which 17 were waited for; matrix products, arithmetic and copies ran while one was open for 5% of the time, Pallas kernels for 16%

commit v1 on v0

--- a/solution.py
+++ b/solution.py
@@ -396,53 +396,38 @@
 
 SHIFTS = (0, -1, 1, 2)
 FAR_FIRST = (3, 1, 2, 0)
-AHEAD = 9
 
 
 def hidden_body(
-    pos_ref, normed, w_hbm, far_a, far_b, hidden, down, w_ref, sems, down_sems
+    pos_ref, normed, w_hbm, far_a, far_b, hidden, down, w_ref, sems
 ):
-    x = pos_ref[0]
     width = w_hbm.shape[3] // 3
-    groups = w_hbm.shape[0]
-    tall = groups // 4
     whole = width // 256
     rest = width - whole * 256
     chunks = 2 * whole
     last = chunks * 256
-    starts = [lax.rem(x + s + 4, 4) for s in SHIFTS]
+    count = iter(range(sems.shape[0]))
+
+    def copy(i, lo, hi, to, at):
+        return pltpu.make_async_copy(
+            w_hbm.at[:, i, :, lo:hi], to.at[:, :, at : at + hi - lo], sems.at[next(count)]
+        )
 
     def pieces(n):
         for part in range(2):
-            for k in range(2):
-                rows = pl.ds(k * (groups // 2), groups // 2)
-                to = w_ref.at[part]
-                if n == chunks:
-                    for i in range(2):
-                        yield pltpu.make_async_copy(
-                            w_hbm.at[rows, i, :, part * width + whole * 256 : (part + 1) * width],
-                            to.at[rows, :, last + i * rest : last + (i + 1) * rest],
-                            sems.at[n, part, 2 * k + i],
-                        )
-                else:
-                    at = part * width + (n % whole) * 256
-                    yield pltpu.make_async_copy(
-                        w_hbm.at[rows, n // whole, :, at : at + 256],
-                        to.at[rows, :, n * 256 : (n + 1) * 256],
-                        sems.at[n, part, k],
-                    )
-
-    def down_pieces(j):
-        rows = pl.ds(starts[j] * tall, tall)
+            to, base = w_ref.at[part], part * width
+            if n == chunks:
+                for i in range(2):
+                    yield copy(i, base + whole * 256, base + width, to, last + i * rest)
+            else:
+                lo = base + n % whole * 256
+                yield copy(n // whole, lo, lo + 256, to, n * 256)
+
+    def down_pieces():
         for i in range(2):
-            for k, (lo, hi, to) in enumerate(
-                ((0, whole * 256, i * whole * 256), (whole * 256, width, last + i * rest))
-            ):
-                yield pltpu.make_async_copy(
-                    w_hbm.at[rows, i, :, 2 * width + lo : 2 * width + hi],
-                    down.at[rows, :, to : to + hi - lo],
-                    down_sems.at[j, i, k],
-                )
+            base = 2 * width
+            yield copy(i, base, base + whole * 256, down, i * whole * 256)
+            yield copy(i, base + whole * 256, base + width, down, last + i * rest)
 
     def begin(copies):
         for each in copies:
@@ -452,22 +437,16 @@
         for each in copies:
             each.wait()
 
-    order = [pieces(n) for n in range(chunks + 1)]
-    order = [list(each) for each in order] + [list(down_pieces(j)) for j in FAR_FIRST]
-    for each in order[:AHEAD]:
+    order = [list(pieces(n)) for n in range(chunks + 1)] + [list(down_pieces())]
+    for each in order:
         begin(each)
     for n in range(chunks + 1):
         finish(order[n])
-        if n + AHEAD < len(order):
-            begin(order[n + AHEAD])
         wide = 256 if n < chunks else 2 * rest
         hidden_chunk(normed, w_ref, hidden, slice(n * 256, n * 256 + wide), wide)
-    for each in order[chunks + 1 + AHEAD :]:
-        begin(each)
-    finish(down_pieces(FAR_FIRST[0]))
-    down_part(hidden, down, starts[FAR_FIRST[0]], far_a, far_b)
-    for j in FAR_FIRST[1:]:
-        finish(down_pieces(j))
+    finish(order[chunks + 1])
+    at = lax.rem(pos_ref[0] + SHIFTS[FAR_FIRST[0]] + 4, 4)
+    down_part(hidden, down, at, far_a, far_b)
 
 
 def near_body(pos_ref, hidden, down, *outs):
@@ -700,8 +679,7 @@
         "hidden",
         scratch=(
             pltpu.VMEM((2, *wide), BF16),
-            pltpu.SemaphoreType.DMA((shard_cols // 3 // 256 * 2 + 1, 2, 4)),
-            pltpu.SemaphoreType.DMA((4, 2, 2)),
+            pltpu.SemaphoreType.DMA((shard_cols // 3 // 256 * 4 + 8,)),
         ),
         spaces=[pltpu.SMEM, pltpu.VMEM, pltpu.HBM],
         limit=20,

time: 156 us -> 156 us (level)
  no operation moved by 1% of the time
where the time goes in v1:
time: 156 us
  starting transfers between devices  48.5 us (31%)
  waiting for transfers between devices  47.9 us (31%)
  Pallas kernels  36.6 us (23%)
  between operations  13.6 us (9%)
  other arithmetic  5.02 us (3%)
  local copies, waits for them, and re-layouts  3.91 us (3%)
    ppermute x25, waiting for transfers between devices, turned(): return lax.ppermute(x, axis, [(i, (i + distance) % n) for i in range(n)])  37.7 us
    ppermute x25, starting transfers between devices, turned(): return lax.ppermute(x, axis, [(i, (i + distance) % n) for i in range(n)])  35.6 us
    pallas_call x10, Pallas kernels, call(): pl.pallas_call(body, out_shape=tuple(((pltpu.HBM if i in spilled else plt...  35.1 us
    all_to_all x1, starting transfers between devices, shards(): rows = lax.all_to_all(total, 'z', 0, 0, tiled=True)  8.9 us
    all_to_all x1, waiting for transfers between devices, shards(): rows = lax.all_to_all(total, 'z', 0, 0, tiled=True)  5.25 us
    ppermute x1, starting transfers between devices, shards(): rim = lax.ppermute(packed, SP, [(i, i + 1) for i in range(count - 1)])  4.01 us
    all_gather x1, waiting for transfers between devices, shards(): all_w = lax.all_gather(own_rows, SP + ('c',), axis=0, tiled=True)  3.82 us
  transfers between devices with their start and end apart: 28, of which 17 were waited for; matrix products, arithmetic and copies ran while one was open for 5% of the time, Pallas kernels for 16%

profile of v1, /device:TPU:1, one launch (start us, length us, event | category | flops | bytes accessed | tf_op | source)
XLA Modules:
  0.0 155.6 jit_solution(6858693912710933762)
XLA Ops:
  6.5 1.7 %pad_maximum_fusion = bf16[64,1920]{1,0:T(8,128)(2,1)} fusion(bf16[64,640]{1,0:T(8,128)(2,1)} %param.37, bf16[64,640]{1,0:T(8,128)(2,1)} %param.36, bf16[64,640]{1,0:T(8,128)(2,1)} %param.35), kind=kLoop, calls=%fused_computation.6 | loop fusion | flops 737280 | bytes 491520 | tf_op jit(solution)/shard_map/concatenate | solution.py:562
  8.3 1.9 %copy.26 = bf16[128,8,2,128]{3,1,2,0:T(8,128)(2,1)} copy(bf16[128,8,2,128]{3,2,1,0:T(2,128)(2,1)} %bitcast.27) | data formatting | bytes 1048576
  10.2 1.6 %pack_rim.1 = bf16[16,640]{1,0:T(8,128)(2,1)} custom-call(bf16[1024,256]{1,0:T(8,128)(2,1)} %bitcast.23, bf16[1024,128]{1,0:T(8,128)(2,1)} %k1_ref.3, bf16[1024,128]{1,0:T(8,128)(2,1)} %q1_ref.3, bf16[64,1024]{1,0:T(8,128)(2,1)} %bitcast.29, bf16[64,1024]{1,0:T(8,128)(2,1)} %bitcast.31), custom_call_target="tpu_custom_call" | custom-call | tf_op jit(solution)/shard_map/pack_rim/pallas_call | solution.py:36
  11.8 4.0 %collective-permute-start = (bf16[16,640]{1,0:T(8,128)(2,1)}, bf16[16,640]{1,0:T(8,128)(2,1)S(1)}, u32[]{:S(2)}, u32[]{:S(2)}) collective-permute-start(bf16[16,640]{1,0:T(8,128)(2,1)} %pack_rim.1), channel_id=1, source_target_pairs={{0,8},{8,16},{16,24},{24,32},{32,40},{40,48},{48,56},{56,64},{64,7... | collective-permute-start | bytes 61448 | tf_op jit(solution)/shard_map/ppermute | solution.py:570
  16.9 7.0 %shard_map.181 = (bf16[1024,256]{1,0:T(8,128)(2,1)S(1)}, bf16[1024,128]{1,0:T(8,128)(2,1)}, bf16[1024,128]{1,0:T(8,128)(2,1)S(1)}, bf16[1024,128]{1,0:T(8,128)(2...) custom-call(f32[2,2]{1,0:T(2,128)S(1)} %copy-done, ...), custom_call_target="tpu_custom_call" | custom-call | tf_op jit(solution)/shard_map/pallas_call | solution.py:541
  23.9 3.2 %collective-permute-start.3 = (bf16[208,128]{1,0:T(8,128)(2,1)S(1)}, bf16[208,128]{1,0:T(8,128)(2,1)S(1)}, u32[]{:S(2)}, u32[]{:S(2)}) collective-permute-start(bf16[208,128]{1,0:T(8,128)(2,1)S(1)} %get-tuple-element.41.own_ref), channel_id=1, source_target_pairs={{0,24},{8,0},{16,8},{24,16},{1,25},{9,1},{17,9},{25,17},{2,26},{10... | collective-permute-start | bytes 159752 | tf_op jit(solution)/shard_map/ppermute | solution.py:491
  28.5 4.0 %collective-permute-done.2.b2_ref = bf16[208,128]{1,0:T(8,128)(2,1)S(1)} collective-permute-done((bf16[208,128]{1,0:T(8,128)(2,1)S(1)}, bf16[208,128]{1,0:T(8,128)(2,1)S(1)}, u32[]{:S(2)}, u32[]{:S(2)}) %collective-permute-start.2) | collective-permute-done | bytes 53280 | tf_op jit(solution)/shard_map/ppermute | solution.py:491
  34.7 8.9 %all-to-all-start = ((bf16[8,208,128]{2,1,0:T(8,128)(2,1)}), bf16[8,208,128]{2,1,0:T(8,128)(2,1)S(1)}, u32[]{:S(2)}, u32[]{:S(2)}) async-start(bf16[8,208,128]{2,1,0:T(8,128)(2,1)} %get-tuple-element.42), calls=%async_computation | async-start | bytes 851968 | tf_op jit(solution)/shard_map/all_to_all | solution.py:615
  44.7 2.5 %collective-permute-start.11 = (bf16[2048,256]{1,0:T(8,128)(2,1)}, bf16[2048,256]{1,0:T(8,128)(2,1)}, u32[]{:S(2)}, u32[]{:S(2)}) collective-permute-start(bf16[2048,256]{1,0:T(8,128)(2,1)} %bitcast.10), channel_id=1, source_target_pairs={{0,1},{1,0},{2,3},{3,2},{4,5},{5,4},{6,7},{7,6},{8,9},{9,8},{10,11... | collective-permute-start | bytes 3145736 | tf_op jit(solution)/shard_map/ppermute | solution.py:491
  48.0 4.6 %shard_map.183.in_ref = f32[1024,256]{1,0:T(8,128)S(1)} custom-call(bf16[1024,256]{1,0:T(8,128)(2,1)S(1)} %get-tuple-element.43.xc_ref, bf16[1024,128]{1,0:T(8,128)(2,1)} %get-tuple-element.44.k1_ref, bf16[1024,128]{1,0:T(8,128)(2,1)S(1)} %get-tuple-element.45.q1_ref, bf16[1024,128]{1,0:T(8,128)(2,1)S(1)} %get-tuple-element.46.kq2_ref, ...), custom_call_target="tpu_custom_call" | custom-call | tf_op jit(solution)/shard_map/pallas_call | solution.py:541
  52.6 5.3 %all-to-all-done.rows_ref = bf16[8,208,128]{2,1,0:T(8,128)(2,1)S(1)} async-done(((bf16[8,208,128]{2,1,0:T(8,128)(2,1)}), bf16[8,208,128]{2,1,0:T(8,128)(2,1)S(1)}, u32[]{:S(2)}, u32[]{:S(2)}) %all-to-all-start) | async-done | bytes 426016 | tf_op jit(solution)/shard_map/all_to_all | solution.py:615
  57.9 4.1 %shard_map.184 = (bf16[512,256]{1,0:T(8,128)(2,1)S(1)}, bf16[512,256]{1,0:T(8,128)(2,1)S(1)}) custom-call(s32[4]{0:T(128)S(1)} %pad_add_fusion.y_ref.pos_ref, f32[1024,256]{1,0:T(8,128)S(1)} %shard_map.183.in_ref, bf16[1024,256]{1,0:T(8,128)(2,1)} %bitcast.25, bf16[1024,128]{1,0:T(8,128)(2,1)S(1)} %get-tuple-element.45.q1_ref, ...), custom_call_target="tpu_custom_call" | custom-call | tf_op jit(solution)/shard_map/pallas_call | solution.py:541
  62.0 3.0 %collective-permute-start.4 = (bf16[512,256]{1,0:T(8,128)(2,1)S(1)}, bf16[512,256]{1,0:T(8,128)(2,1)S(1)}, u32[]{:S(2)}, u32[]{:S(2)}) collective-permute-start(bf16[512,256]{1,0:T(8,128)(2,1)S(1)} %get-tuple-element.56), channel_id=1, source_target_pairs={{0,1},{1,0},{2,3},{3,2},{4,5},{5,4},{6,7},{7,6},{8,9},{9,8},{10,11... | collective-permute-start | bytes 786440 | tf_op jit(solution)/shard_map/ppermute | solution.py:491
  66.4 2.4 %collective-permute-start.8 = (bf16[512,256]{1,0:T(8,128)(2,1)S(1)}, bf16[512,256]{1,0:T(8,128)(2,1)S(1)}, u32[]{:S(2)}, u32[]{:S(2)}) collective-permute-start(bf16[512,256]{1,0:T(8,128)(2,1)S(1)} %collective-permute-done.4.refs_1_), channel_id=1, source_target_pairs={{0,6},{2,0},{4,2},{6,4},{1,7},{3,1},{5,3},{7,5},{8,14},{10,8},{12,... | collective-permute-start | bytes 786440 | tf_op jit(solution)/shard_map/ppermute | solution.py:491
  70.4 3.6 %collective-permute-done.5.refs_2_ = bf16[512,256]{1,0:T(8,128)(2,1)S(1)} collective-permute-done((bf16[512,256]{1,0:T(8,128)(2,1)S(1)}, bf16[512,256]{1,0:T(8,128)(2,1)S(1)}, u32[]{:S(2)}, u32[]{:S(2)}) %collective-permute-start.5) | collective-permute-done | bytes 262176 | tf_op jit(solution)/shard_map/ppermute | solution.py:491
  74.0 3.5 %collective-permute-start.10 = (bf16[512,256]{1,0:T(8,128)(2,1)S(1)}, bf16[512,256]{1,0:T(8,128)(2,1)S(1)}, u32[]{:S(2)}, u32[]{:S(2)}) collective-permute-start(bf16[512,256]{1,0:T(8,128)(2,1)S(1)} %collective-permute-done.8.refs_5_), channel_id=1, source_target_pairs={{0,6},{2,0},{4,2},{6,4},{1,7},{3,1},{5,3},{7,5},{8,14},{10,8},{12,... | collective-permute-start | bytes 786440 | tf_op jit(solution)/shard_map/ppermute | solution.py:491
  77.5 3.0 %maximum_select_fusion.refs_8_ = bf16[2048,512]{1,0:T(8,128)(2,1)S(1)} fusion(bf16[2048,256]{1,0:T(8,128)(2,1)} %collective-permute-done.11, bf16[2048,256]{1,0:T(8,128)(2,1)} %bitcast.10, pred[]{:T(512)S(6)} %eq.4), kind=kLoop, calls=%fused_computation | loop fusion | flops 9437184 | bytes 4194305 | tf_op jit(solution)/shard_map/jit(_where)/select_n | solution.py:641
  80.5 4.7 %collective-permute-done.9.refs_6_ = bf16[512,256]{1,0:T(8,128)(2,1)S(1)} collective-permute-done((bf16[512,256]{1,0:T(8,128)(2,1)S(1)}, bf16[512,256]{1,0:T(8,128)(2,1)S(1)}, u32[]{:S(2)}, u32[]{:S(2)}) %collective-permute-start.9) | collective-permute-done | bytes 262176 | tf_op jit(solution)/shard_map/ppermute | solution.py:491
  85.3 2.1 %shard_map.185 = (bf16[256,512]{1,0:T(8,128)(2,1)S(1)}, bf16[256,512]{1,0:T(8,128)(2,1)S(1)}) custom-call(s32[4]{0:T(128)S(1)} %pad_add_fusion.y_ref.pos_ref, bf16[512,256]{1,0:T(8,128)(2,1)S(1)} %get-tuple-element.55.refs_0_, bf16[512,256]{1,0:T(8,128)(2,1)S(1)} %collective-permute-done.4.refs_1_, bf16[512,256]{1,0:T(8,128)(2,1)S(1)} %collective-permute-done.5.refs_2_, ...), custom_call_target="tpu_custom_call" | custom-call | tf_op jit(solution)/shard_map/pallas_call | solution.py:541
  88.3 2.7 %collective-permute-start.17 = (bf16[256,512]{1,0:T(8,128)(2,1)S(1)}, bf16[256,512]{1,0:T(8,128)(2,1)S(1)}, u32[]{:S(2)}, u32[]{:S(2)}) collective-permute-start(bf16[256,512]{1,0:T(8,128)(2,1)S(1)} %get-tuple-element.60.refs_4_.sb_ref), channel_id=1, source_target_pairs={{0,6},{2,0},{4,2},{6,4},{1,7},{3,1},{5,3},{7,5},{8,14},{10,8},{12,... | collective-permute-start | bytes 786440 | tf_op jit(solution)/shard_map/ppermute | solution.py:491
  92.5 4.1 %collective-permute-done.13.refs_1_ = bf16[256,512]{1,0:T(8,128)(2,1)S(1)} collective-permute-done((bf16[256,512]{1,0:T(8,128)(2,1)S(1)}, bf16[256,512]{1,0:T(8,128)(2,1)S(1)}, u32[]{:S(2)}, u32[]{:S(2)}) %collective-permute-start.13) | collective-permute-done | bytes 262176 | tf_op jit(solution)/shard_map/ppermute | solution.py:491
  96.6 2.7 %collective-permute-start.18 = (bf16[256,512]{1,0:T(8,128)(2,1)S(1)}, bf16[256,512]{1,0:T(8,128)(2,1)S(1)}, u32[]{:S(2)}, u32[]{:S(2)}) collective-permute-start(bf16[256,512]{1,0:T(8,128)(2,1)S(1)} %collective-permute-done.17.refs_6_), channel_id=1, source_target_pairs={{0,6},{2,0},{4,2},{6,4},{1,7},{3,1},{5,3},{7,5},{8,14},{10,8},{12,... | collective-permute-start | bytes 786440 | tf_op jit(solution)/shard_map/ppermute | solution.py:491
  99.3 1.9 %collective-permute-done.14.refs_2_ = bf16[256,512]{1,0:T(8,128)(2,1)S(1)} collective-permute-done((bf16[256,512]{1,0:T(8,128)(2,1)S(1)}, bf16[256,512]{1,0:T(8,128)(2,1)S(1)}, u32[]{:S(2)}, u32[]{:S(2)}) %collective-permute-start.14) | collective-permute-done | bytes 262176 | tf_op jit(solution)/shard_map/ppermute | solution.py:491
  102.2 5.6 %collective-permute-done.15.refs_3_ = bf16[256,512]{1,0:T(8,128)(2,1)S(1)} collective-permute-done((bf16[256,512]{1,0:T(8,128)(2,1)S(1)}, bf16[256,512]{1,0:T(8,128)(2,1)S(1)}, u32[]{:S(2)}, u32[]{:S(2)}) %collective-permute-start.15) | collective-permute-done | bytes 262176 | tf_op jit(solution)/shard_map/ppermute | solution.py:491
  109.3 3.8 %all-gather.2.cloned.1.call-done = bf16[4096,1920]{1,0:T(8,128)(2,1)} async-done(((bf16[64,1920]{1,0:T(8,128)(2,1)}), bf16[4096,1920]{1,0:T(8,128)(2,1)}) %all-gather.2.cloned.1.call-update) | async-done | bytes 15728656 | tf_op jit(solution)/shard_map/all_gather | solution.py:565
  113.1 9.5 %shard_map.187 = (bf16[256,512]{1,0:T(8,128)(2,1)S(1)}, bf16[256,512]{1,0:T(8,128)(2,1)S(1)}, bf16[512,1280]{1,0:T(8,128)(2,1)S(1)}, bf16[32,64,1280]{2,1,0:T(8,128)(2,1)S(1)}) custom-call(s32[4]{0:T(128)S(1)} %pad_add_fusion.y_ref.pos_ref, bf16[512,2048]{1,0:T(8,128)(2,1)S(1)} %shard_map.186.normed, bf16[32,2,64,1920]{3,2,1,0:T(8,128)(2,1)} %bitcast.22), custom_call_target="tpu_custom_call" | custom-call | tf_op jit(solution)/shard_map/pallas_call | solution.py:541
  125.7 2.8 %shard_map.188 = (bf16[256,512]{1,0:T(8,128)(2,1)S(1)}, bf16[256,512]{1,0:T(8,128)(2,1)S(1)}, bf16[256,512]{1,0:T(8,128)(2,1)S(1)}, bf16[256,512]{1,0:T(8,128)(2...) custom-call(s32[4]{0:T(128)S(1)} %pad_add_fusion.y_ref.pos_ref, ...), custom_call_target="tpu_custom_call" | custom-call | tf_op jit(solution)/shard_map/pallas_call | solution.py:541
  130.0 1.8 %collective-permute-done.19 = bf16[256,512]{1,0:T(8,128)(2,1)S(1)} collective-permute-done((bf16[256,512]{1,0:T(8,128)(2,1)S(1)}, bf16[256,512]{1,0:T(8,128)(2,1)S(1)}, u32[]{:S(2)}, u32[]{:S(2)}) %collective-permute-start.19) | collective-permute-done | bytes 262176 | tf_op jit(solution)/shard_map/ppermute | solution.py:491
  132.0 2.7 %collective-permute-start.24 = (bf16[256,512]{1,0:T(8,128)(2,1)S(1)}, bf16[256,512]{1,0:T(8,128)(2,1)S(1)}, u32[]{:S(2)}, u32[]{:S(2)}) collective-permute-start(bf16[256,512]{1,0:T(8,128)(2,1)S(1)} %add_convert_fusion), channel_id=1, source_target_pairs={{0,6},{2,0},{4,2},{6,4},{1,7},{3,1},{5,3},{7,5},{8,14},{10,8},{12,... | collective-permute-start | bytes 786440 | tf_op jit(solution)/shard_map/ppermute | solution.py:491
  134.8 2.3 %collective-permute-done.21.ra_ref = bf16[256,512]{1,0:T(8,128)(2,1)S(1)} collective-permute-done((bf16[256,512]{1,0:T(8,128)(2,1)S(1)}, bf16[256,512]{1,0:T(8,128)(2,1)S(1)}, u32[]{:S(2)}, u32[]{:S(2)}) %collective-permute-start.21) | collective-permute-done | bytes 262176 | tf_op jit(solution)/shard_map/ppermute | solution.py:491
  137.7 5.6 %collective-permute-done.20.la_ref = bf16[256,512]{1,0:T(8,128)(2,1)S(1)} collective-permute-done((bf16[256,512]{1,0:T(8,128)(2,1)S(1)}, bf16[256,512]{1,0:T(8,128)(2,1)S(1)}, u32[]{:S(2)}, u32[]{:S(2)}) %collective-permute-start.20) | collective-permute-done | bytes 262176 | tf_op jit(solution)/shard_map/ppermute | solution.py:491
  144.2 2.0 %collective-permute-start.25 = (bf16[512,256]{1,0:T(8,128)(2,1)S(1)}, bf16[512,256]{1,0:T(8,128)(2,1)S(1)}, u32[]{:S(2)}, u32[]{:S(2)}) collective-permute-start(bf16[512,256]{1,0:T(8,128)(2,1)S(1)} %get-tuple-element.72), channel_id=1, source_target_pairs={{0,1},{1,0},{2,3},{3,2},{4,5},{5,4},{6,7},{7,6},{8,9},{9,8},{10,11... | collective-permute-start | bytes 786440 | tf_op jit(solution)/shard_map/ppermute | solution.py:491
  (54 shorter events, 23.5 us)
Async XLA Ops:
  6.5 10.4 %copy-start = (f32[2,2]{1,0:T(2,128)S(1)}, f32[2,2]{1,0:T(2,128)}, u32[]{:S(2)}) copy-start(f32[2,2]{1,0:T(2,128)} %rate_ref.1) | copy-start | bytes 52
  6.5 106.6 %all-gather.2.cloned.1.call-start = ((), (), s32[]{:S(2)}) async-start(), calls=%async_computation.1 | async-start | bytes 15974400 | tf_op jit(solution)/shard_map/all_gather | solution.py:565
  10.2 33.4 %copy-start.1 = (bf16[2,1024,256]{2,1,0:T(8,128)(2,1)S(1)}, bf16[2,1024,256]{2,1,0:T(8,128)(2,1)}, u32[]{:S(2)}) copy-start(bf16[2,1024,256]{2,1,0:T(8,128)(2,1)} %param.32) | copy-start | bytes 3145732
  11.8 5.1 %collective-permute-start = (bf16[16,640]{1,0:T(8,128)(2,1)}, bf16[16,640]{1,0:T(8,128)(2,1)S(1)}, u32[]{:S(2)}, u32[]{:S(2)}) collective-permute-start(bf16[16,640]{1,0:T(8,128)(2,1)} %pack_rim.1), channel_id=1, source_target_pairs={{0,8},{8,16},{16,24},{24,32},{32,40},{40,48},{48,56},{56,64},{64,7... | collective-permute-start | bytes 61448 | tf_op jit(solution)/shard_map/ppermute | solution.py:570
  16.9 30.3 %copy-start.3 = (bf16[1024,2,128]{2,1,0:T(2,128)(2,1)S(1)}, bf16[1024,2,128]{2,1,0:T(2,128)(2,1)}, u32[]{:S(2)}) copy-start(bf16[1024,2,128]{2,1,0:T(2,128)(2,1)} %param.20) | copy-start | bytes 1572868
  23.9 4.6 %collective-permute-start.3 = (bf16[208,128]{1,0:T(8,128)(2,1)S(1)}, bf16[208,128]{1,0:T(8,128)(2,1)S(1)}, u32[]{:S(2)}, u32[]{:S(2)}) collective-permute-start(bf16[208,128]{1,0:T(8,128)(2,1)S(1)} %get-tuple-element.41.own_ref), channel_id=1, source_target_pairs={{0,24},{8,0},{16,8},{24,16},{1,25},{9,1},{17,9},{25,17},{2,26},{10... | collective-permute-start | bytes 159752 | tf_op jit(solution)/shard_map/ppermute | solution.py:491
  27.0 5.5 %collective-permute-start.2 = (bf16[208,128]{1,0:T(8,128)(2,1)S(1)}, bf16[208,128]{1,0:T(8,128)(2,1)S(1)}, u32[]{:S(2)}, u32[]{:S(2)}) collective-permute-start(bf16[208,128]{1,0:T(8,128)(2,1)S(1)} %get-tuple-element.41.own_ref), channel_id=1, source_target_pairs={{0,16},{8,24},{16,0},{24,8},{1,17},{9,25},{17,1},{25,9},{2,18},{10... | collective-permute-start | bytes 159752 | tf_op jit(solution)/shard_map/ppermute | solution.py:491
  27.4 6.0 %collective-permute-start.1 = (bf16[208,128]{1,0:T(8,128)(2,1)S(1)}, bf16[208,128]{1,0:T(8,128)(2,1)S(1)}, u32[]{:S(2)}, u32[]{:S(2)}) collective-permute-start(bf16[208,128]{1,0:T(8,128)(2,1)S(1)} %get-tuple-element.41.own_ref), channel_id=1, source_target_pairs={{0,8},{8,16},{16,24},{24,0},{1,9},{9,17},{17,25},{25,1},{2,10},{10... | collective-permute-start | bytes 159752 | tf_op jit(solution)/shard_map/ppermute | solution.py:491
  34.7 23.2 %all-to-all-start = ((bf16[8,208,128]{2,1,0:T(8,128)(2,1)}), bf16[8,208,128]{2,1,0:T(8,128)(2,1)S(1)}, u32[]{:S(2)}, u32[]{:S(2)}) async-start(bf16[8,208,128]{2,1,0:T(8,128)(2,1)} %get-tuple-element.42), calls=%async_computation | async-start | bytes 851968 | tf_op jit(solution)/shard_map/all_to_all | solution.py:615
  44.7 32.9 %collective-permute-start.11 = (bf16[2048,256]{1,0:T(8,128)(2,1)}, bf16[2048,256]{1,0:T(8,128)(2,1)}, u32[]{:S(2)}, u32[]{:S(2)}) collective-permute-start(bf16[2048,256]{1,0:T(8,128)(2,1)} %bitcast.10), channel_id=1, source_target_pairs={{0,1},{1,0},{2,3},{3,2},{4,5},{5,4},{6,7},{7,6},{8,9},{9,8},{10,11... | collective-permute-start | bytes 3145736 | tf_op jit(solution)/shard_map/ppermute | solution.py:491
  52.6 12.4 %copy-start.2 = (bf16[1024,256]{1,0:T(8,128)(2,1)S(1)}, bf16[1024,256]{1,0:T(8,128)(2,1)}, u32[]{:S(2)}) copy-start(bf16[1024,256]{1,0:T(8,128)(2,1)} %param.33) | copy-start | bytes 1572868
  62.0 4.4 %collective-permute-start.4 = (bf16[512,256]{1,0:T(8,128)(2,1)S(1)}, bf16[512,256]{1,0:T(8,128)(2,1)S(1)}, u32[]{:S(2)}, u32[]{:S(2)}) collective-permute-start(bf16[512,256]{1,0:T(8,128)(2,1)S(1)} %get-tuple-element.56), channel_id=1, source_target_pairs={{0,1},{1,0},{2,3},{3,2},{4,5},{5,4},{6,7},{7,6},{8,9},{9,8},{10,11... | collective-permute-start | bytes 786440 | tf_op jit(solution)/shard_map/ppermute | solution.py:491
  65.0 3.7 %collective-permute-start.12 = (bf16[512,256]{1,0:T(8,128)(2,1)S(1)}, bf16[512,256]{1,0:T(8,128)(2,1)S(1)}, u32[]{:S(2)}, u32[]{:S(2)}) collective-permute-start(bf16[512,256]{1,0:T(8,128)(2,1)S(1)} %get-tuple-element.74), channel_id=1, source_target_pairs={{0,1},{1,0},{2,3},{3,2},{4,5},{5,4},{6,7},{7,6},{8,9},{9,8},{10,11... | collective-permute-start | bytes 786440 | tf_op jit(solution)/shard_map/ppermute | solution.py:491
  65.2 8.8 %collective-permute-start.5 = (bf16[512,256]{1,0:T(8,128)(2,1)S(1)}, bf16[512,256]{1,0:T(8,128)(2,1)S(1)}, u32[]{:S(2)}, u32[]{:S(2)}) collective-permute-start(bf16[512,256]{1,0:T(8,128)(2,1)S(1)} %get-tuple-element.55.refs_0_), channel_id=1, source_target_pairs={{0,2},{2,4},{4,6},{6,0},{1,3},{3,5},{5,7},{7,1},{8,10},{10,12},{12... | collective-permute-start | bytes 786440 | tf_op jit(solution)/shard_map/ppermute | solution.py:491
  66.4 7.7 %collective-permute-start.8 = (bf16[512,256]{1,0:T(8,128)(2,1)S(1)}, bf16[512,256]{1,0:T(8,128)(2,1)S(1)}, u32[]{:S(2)}, u32[]{:S(2)}) collective-permute-start(bf16[512,256]{1,0:T(8,128)(2,1)S(1)} %collective-permute-done.4.refs_1_), channel_id=1, source_target_pairs={{0,6},{2,0},{4,2},{6,4},{1,7},{3,1},{5,3},{7,5},{8,14},{10,8},{12,... | collective-permute-start | bytes 786440 | tf_op jit(solution)/shard_map/ppermute | solution.py:491
  68.9 11.6 %collective-permute-start.7 = (bf16[512,256]{1,0:T(8,128)(2,1)S(1)}, bf16[512,256]{1,0:T(8,128)(2,1)S(1)}, u32[]{:S(2)}, u32[]{:S(2)}) collective-permute-start(bf16[512,256]{1,0:T(8,128)(2,1)S(1)} %get-tuple-element.55.refs_0_), channel_id=1, source_target_pairs={{0,6},{2,0},{4,2},{6,4},{1,7},{3,1},{5,3},{7,5},{8,14},{10,8},{12,... | collective-permute-start | bytes 786440 | tf_op jit(solution)/shard_map/ppermute | solution.py:491
  69.5 11.0 %collective-permute-start.6 = (bf16[512,256]{1,0:T(8,128)(2,1)S(1)}, bf16[512,256]{1,0:T(8,128)(2,1)S(1)}, u32[]{:S(2)}, u32[]{:S(2)}) collective-permute-start(bf16[512,256]{1,0:T(8,128)(2,1)S(1)} %collective-permute-done.4.refs_1_), channel_id=1, source_target_pairs={{0,2},{2,4},{4,6},{6,0},{1,3},{3,5},{5,7},{7,1},{8,10},{10,12},{12... | collective-permute-start | bytes 786440 | tf_op jit(solution)/shard_map/ppermute | solution.py:491
  74.0 11.2 %collective-permute-start.9 = (bf16[512,256]{1,0:T(8,128)(2,1)S(1)}, bf16[512,256]{1,0:T(8,128)(2,1)S(1)}, u32[]{:S(2)}, u32[]{:S(2)}) collective-permute-start(bf16[512,256]{1,0:T(8,128)(2,1)S(1)} %collective-permute-done.5.refs_2_), channel_id=1, source_target_pairs={{0,2},{2,4},{4,6},{6,0},{1,3},{3,5},{5,7},{7,1},{8,10},{10,12},{12... | collective-permute-start | bytes 786440 | tf_op jit(solution)/shard_map/ppermute | solution.py:491
  74.0 11.2 %collective-permute-start.10 = (bf16[512,256]{1,0:T(8,128)(2,1)S(1)}, bf16[512,256]{1,0:T(8,128)(2,1)S(1)}, u32[]{:S(2)}, u32[]{:S(2)}) collective-permute-start(bf16[512,256]{1,0:T(8,128)(2,1)S(1)} %collective-permute-done.8.refs_5_), channel_id=1, source_target_pairs={{0,6},{2,0},{4,2},{6,4},{1,7},{3,1},{5,3},{7,5},{8,14},{10,8},{12,... | collective-permute-start | bytes 786440 | tf_op jit(solution)/shard_map/ppermute | solution.py:491
  87.3 9.3 %collective-permute-start.13 = (bf16[256,512]{1,0:T(8,128)(2,1)S(1)}, bf16[256,512]{1,0:T(8,128)(2,1)S(1)}, u32[]{:S(2)}, u32[]{:S(2)}) collective-permute-start(bf16[256,512]{1,0:T(8,128)(2,1)S(1)} %get-tuple-element.59.refs_0_.sa_ref), channel_id=1, source_target_pairs={{0,2},{2,4},{4,6},{6,0},{1,3},{3,5},{5,7},{7,1},{8,10},{10,12},{12... | collective-permute-start | bytes 786440 | tf_op jit(solution)/shard_map/ppermute | solution.py:491
  88.3 8.3 %collective-permute-start.17 = (bf16[256,512]{1,0:T(8,128)(2,1)S(1)}, bf16[256,512]{1,0:T(8,128)(2,1)S(1)}, u32[]{:S(2)}, u32[]{:S(2)}) collective-permute-start(bf16[256,512]{1,0:T(8,128)(2,1)S(1)} %get-tuple-element.60.refs_4_.sb_ref), channel_id=1, source_target_pairs={{0,6},{2,0},{4,2},{6,4},{1,7},{3,1},{5,3},{7,5},{8,14},{10,8},{12,... | collective-permute-start | bytes 786440 | tf_op jit(solution)/shard_map/ppermute | solution.py:491
  91.0 10.2 %collective-permute-start.14 = (bf16[256,512]{1,0:T(8,128)(2,1)S(1)}, bf16[256,512]{1,0:T(8,128)(2,1)S(1)}, u32[]{:S(2)}, u32[]{:S(2)}) collective-permute-start(bf16[256,512]{1,0:T(8,128)(2,1)S(1)} %get-tuple-element.59.refs_0_.sa_ref), channel_id=1, source_target_pairs={{0,6},{2,0},{4,2},{6,4},{1,7},{3,1},{5,3},{7,5},{8,14},{10,8},{12,... | collective-permute-start | bytes 786440 | tf_op jit(solution)/shard_map/ppermute | solution.py:491
  92.4 9.8 %collective-permute-start.16 = (bf16[256,512]{1,0:T(8,128)(2,1)S(1)}, bf16[256,512]{1,0:T(8,128)(2,1)S(1)}, u32[]{:S(2)}, u32[]{:S(2)}) collective-permute-start(bf16[256,512]{1,0:T(8,128)(2,1)S(1)} %get-tuple-element.60.refs_4_.sb_ref), channel_id=1, source_target_pairs={{0,2},{2,4},{4,6},{6,0},{1,3},{3,5},{5,7},{7,1},{8,10},{10,12},{12... | collective-permute-start | bytes 786440 | tf_op jit(solution)/shard_map/ppermute | solution.py:491
  96.6 11.2 %collective-permute-start.15 = (bf16[256,512]{1,0:T(8,128)(2,1)S(1)}, bf16[256,512]{1,0:T(8,128)(2,1)S(1)}, u32[]{:S(2)}, u32[]{:S(2)}) collective-permute-start(bf16[256,512]{1,0:T(8,128)(2,1)S(1)} %collective-permute-done.13.refs_1_), channel_id=1, source_target_pairs={{0,2},{2,4},{4,6},{6,0},{1,3},{3,5},{5,7},{7,1},{8,10},{10,12},{12... | collective-permute-start | bytes 786440 | tf_op jit(solution)/shard_map/ppermute | solution.py:491
  96.6 11.2 %collective-permute-start.18 = (bf16[256,512]{1,0:T(8,128)(2,1)S(1)}, bf16[256,512]{1,0:T(8,128)(2,1)S(1)}, u32[]{:S(2)}, u32[]{:S(2)}) collective-permute-start(bf16[256,512]{1,0:T(8,128)(2,1)S(1)} %collective-permute-done.17.refs_6_), channel_id=1, source_target_pairs={{0,6},{2,0},{4,2},{6,4},{1,7},{3,1},{5,3},{7,5},{8,14},{10,8},{12,... | collective-permute-start | bytes 786440 | tf_op jit(solution)/shard_map/ppermute | solution.py:491
  122.7 9.1 %collective-permute-start.19 = (bf16[256,512]{1,0:T(8,128)(2,1)S(1)}, bf16[256,512]{1,0:T(8,128)(2,1)S(1)}, u32[]{:S(2)}, u32[]{:S(2)}) collective-permute-start(bf16[256,512]{1,0:T(8,128)(2,1)S(1)} %get-tuple-element.65), channel_id=1, source_target_pairs={{0,2},{2,4},{4,6},{6,0},{1,3},{3,5},{5,7},{7,1},{8,10},{10,12},{12... | collective-permute-start | bytes 786440 | tf_op jit(solution)/shard_map/ppermute | solution.py:491
  124.2 7.8 %collective-permute-start.23 = (bf16[256,512]{1,0:T(8,128)(2,1)S(1)}, bf16[256,512]{1,0:T(8,128)(2,1)S(1)}, u32[]{:S(2)}, u32[]{:S(2)}) collective-permute-start(bf16[256,512]{1,0:T(8,128)(2,1)S(1)} %get-tuple-element.70), channel_id=1, source_target_pairs={{0,6},{2,0},{4,2},{6,4},{1,7},{3,1},{5,3},{7,5},{8,14},{10,8},{12,... | collective-permute-start | bytes 786440 | tf_op jit(solution)/shard_map/ppermute | solution.py:491
  128.4 8.7 %collective-permute-start.21 = (bf16[256,512]{1,0:T(8,128)(2,1)S(1)}, bf16[256,512]{1,0:T(8,128)(2,1)S(1)}, u32[]{:S(2)}, u32[]{:S(2)}) collective-permute-start(bf16[256,512]{1,0:T(8,128)(2,1)S(1)} %get-tuple-element.66), channel_id=1, source_target_pairs={{0,6},{2,0},{4,2},{6,4},{1,7},{3,1},{5,3},{7,5},{8,14},{10,8},{12,... | collective-permute-start | bytes 786440 | tf_op jit(solution)/shard_map/ppermute | solution.py:491
  129.7 8.0 %collective-permute-start.22 = (bf16[256,512]{1,0:T(8,128)(2,1)S(1)}, bf16[256,512]{1,0:T(8,128)(2,1)S(1)}, u32[]{:S(2)}, u32[]{:S(2)}) collective-permute-start(bf16[256,512]{1,0:T(8,128)(2,1)S(1)} %get-tuple-element.68), channel_id=1, source_target_pairs={{0,2},{2,4},{4,6},{6,0},{1,3},{3,5},{5,7},{7,1},{8,10},{10,12},{12... | collective-permute-start | bytes 786440 | tf_op jit(solution)/shard_map/ppermute | solution.py:491
  131.9 11.4 %collective-permute-start.20 = (bf16[256,512]{1,0:T(8,128)(2,1)S(1)}, bf16[256,512]{1,0:T(8,128)(2,1)S(1)}, u32[]{:S(2)}, u32[]{:S(2)}) collective-permute-start(bf16[256,512]{1,0:T(8,128)(2,1)S(1)} %add_convert_fusion.1), channel_id=1, source_target_pairs={{0,2},{2,4},{4,6},{6,0},{1,3},{3,5},{5,7},{7,1},{8,10},{10,12},{12... | collective-permute-start | bytes 786440 | tf_op jit(solution)/shard_map/ppermute | solution.py:491
  132.0 11.3 %collective-permute-start.24 = (bf16[256,512]{1,0:T(8,128)(2,1)S(1)}, bf16[256,512]{1,0:T(8,128)(2,1)S(1)}, u32[]{:S(2)}, u32[]{:S(2)}) collective-permute-start(bf16[256,512]{1,0:T(8,128)(2,1)S(1)} %add_convert_fusion), channel_id=1, source_target_pairs={{0,6},{2,0},{4,2},{6,4},{1,7},{3,1},{5,3},{7,5},{8,14},{10,8},{12,... | collective-permute-start | bytes 786440 | tf_op jit(solution)/shard_map/ppermute | solution.py:491
  144.2 3.2 %collective-permute-start.25 = (bf16[512,256]{1,0:T(8,128)(2,1)S(1)}, bf16[512,256]{1,0:T(8,128)(2,1)S(1)}, u32[]{:S(2)}, u32[]{:S(2)}) collective-permute-start(bf16[512,256]{1,0:T(8,128)(2,1)S(1)} %get-tuple-element.72), channel_id=1, source_target_pairs={{0,1},{1,0},{2,3},{3,2},{4,5},{5,4},{6,7},{7,6},{8,9},{9,8},{10,11... | collective-permute-start | bytes 786440 | tf_op jit(solution)/shard_map/ppermute | solution.py:491
Sparse Core Ops, SparseCore 0:
  10.1 103.0 all-gather.1

commit v2 on v1

--- a/solution.py
+++ b/solution.py
@@ -1,3 +1,5 @@
+import functools
+
 import jax
 import jax.numpy as jnp
 from jax import lax
@@ -456,21 +458,21 @@
 
 
 def last_body(
-    pos_ref, sa_ref, pa_ref, la_ref, ra_ref, sb_ref, pb_ref, lb_ref, rb_ref, mine_ref, theirs_ref
+    other, pos_ref, sa_ref, pa_ref, la_ref, ra_ref, sb_ref, pb_ref, lb_ref, rb_ref, out_ref
 ):
     c = pos_ref[1]
     size = sa_ref.shape[0]
+    lanes = pl.ds(pl.multiple_of((1 - c if other else c) * 256, 256), 256)
     parts = ((sa_ref, pa_ref, la_ref, ra_ref), (sb_ref, pb_ref, lb_ref, rb_ref))
     for k, (s_ref, p_ref, left_ref, right_ref) in enumerate(parts):
-        at = slice(k * size, (k + 1) * size)
-        for ref, who in ((theirs_ref, 1 - c), (mine_ref, c)):
-            lanes = pl.ds(pl.multiple_of(who * 256, 256), 256)
-            total = (
-                p_ref[:, lanes].astype(F32)
-                + left_ref[:, lanes].astype(F32)
-                + right_ref[:, lanes].astype(F32)
-            )
-            ref[at, :] = (s_ref[:, lanes].astype(F32) + 0.5 * total).astype(BF16)
+        total = (
+            p_ref[:, lanes].astype(F32)
+            + left_ref[:, lanes].astype(F32)
+            + right_ref[:, lanes].astype(F32)
+        )
+        out_ref[k * size : (k + 1) * size, :] = (
+            s_ref[:, lanes].astype(F32) + 0.5 * total
+        ).astype(BF16)
 
 
 def join_body(pos_ref, mine_ref, other_ref, out_ref, sems):
@@ -699,14 +701,19 @@
     left_a = turned(sum_a, "x", 1)
     sum_b = (pb1.astype(F32) + far_b.astype(F32)).astype(BF16)
     right_b = turned(sum_b, "x", -1)
-    mine, theirs = call(
-        last_body,
-        (shape((half, 256), BF16),) * 2,
-        (pos, stream_a, pa0, left_a, right_a, stream_b, pb0, left_b, right_b),
-        "last",
-        spaces=[pltpu.SMEM] + [pltpu.VMEM] * 8,
-    )
+
+    def last(other, name):
+        return call(
+            functools.partial(last_body, other),
+            shape((half, 256), BF16),
+            (pos, stream_a, pa0, left_a, right_a, stream_b, pb0, left_b, right_b),
+            name,
+            spaces=[pltpu.SMEM] + [pltpu.VMEM] * 8,
+        )
+
+    theirs = last(True, "theirs")
     other = turned(theirs, "c", 1)
+    mine = last(False, "mine")
     return call(
         join_body,
         shape((length, 256), BF16),

time: 156 us -> 156 us (level)
    pallas_call x10 -> x11, Pallas kernels: 35.1 us -> 35.6 us  [call(): pl.pallas_call(body, out_shape=tuple(((pltpu.HBM if i in spilled else plt...]
where the time goes in v2:
time: 156 us
  starting transfers between devices  48.2 us (31%)
  waiting for transfers between devices  47.7 us (31%)
  Pallas kernels  37.2 us (24%)
  between operations  13.6 us (9%)
  other arithmetic  5 us (3%)
  local copies, waits for them, and re-layouts  3.9 us (2%)
    ppermute x25, waiting for transfers between devices, turned(): return lax.ppermute(x, axis, [(i, (i + distance) % n) for i in range(n)])  37 us
    pallas_call x11, Pallas kernels, call(): pl.pallas_call(body, out_shape=tuple(((pltpu.HBM if i in spilled else plt...  35.6 us
    ppermute x25, starting transfers between devices, turned(): return lax.ppermute(x, axis, [(i, (i + distance) % n) for i in range(n)])  35.2 us
    all_to_all x1, starting transfers between devices, shards(): rows = lax.all_to_all(total, 'z', 0, 0, tiled=True)  8.9 us
    all_to_all x1, waiting for transfers between devices, shards(): rows = lax.all_to_all(total, 'z', 0, 0, tiled=True)  5.66 us
    ppermute x1, starting transfers between devices, shards(): rim = lax.ppermute(packed, SP, [(i, i + 1) for i in range(count - 1)])  4.01 us
    all_gather x1, waiting for transfers between devices, shards(): all_w = lax.all_gather(own_rows, SP + ('c',), axis=0, tiled=True)  3.94 us
  transfers between devices with their start and end apart: 28, of which 17 were waited for; matrix products, arithmetic and copies ran while one was open for 5% of the time, Pallas kernels for 16%

profile of v2, /device:TPU:1, one launch (start us, length us, event | category | flops | bytes accessed | tf_op | source)
XLA Modules:
  0.0 155.5 jit_solution(4667908536327343228)
XLA Ops:
  6.5 1.7 %pad_maximum_fusion = bf16[64,1920]{1,0:T(8,128)(2,1)} fusion(bf16[64,640]{1,0:T(8,128)(2,1)} %param.37, bf16[64,640]{1,0:T(8,128)(2,1)} %param.36, bf16[64,640]{1,0:T(8,128)(2,1)} %param.35), kind=kLoop, calls=%fused_computation.6 | loop fusion | flops 737280 | bytes 491520 | tf_op jit(solution)/shard_map/concatenate | solution.py:564
  8.3 1.9 %copy.26 = bf16[128,8,2,128]{3,1,2,0:T(8,128)(2,1)} copy(bf16[128,8,2,128]{3,2,1,0:T(2,128)(2,1)} %bitcast.27) | data formatting | bytes 1048576
  10.2 1.6 %pack_rim.1 = bf16[16,640]{1,0:T(8,128)(2,1)} custom-call(bf16[1024,256]{1,0:T(8,128)(2,1)} %bitcast.23, bf16[1024,128]{1,0:T(8,128)(2,1)} %k1_ref.3, bf16[1024,128]{1,0:T(8,128)(2,1)} %q1_ref.3, bf16[64,1024]{1,0:T(8,128)(2,1)} %bitcast.29, bf16[64,1024]{1,0:T(8,128)(2,1)} %bitcast.31), custom_call_target="tpu_custom_call" | custom-call | tf_op jit(solution)/shard_map/pack_rim/pallas_call | solution.py:38
  11.8 4.0 %collective-permute-start = (bf16[16,640]{1,0:T(8,128)(2,1)}, bf16[16,640]{1,0:T(8,128)(2,1)S(1)}, u32[]{:S(2)}, u32[]{:S(2)}) collective-permute-start(bf16[16,640]{1,0:T(8,128)(2,1)} %pack_rim.1), channel_id=1, source_target_pairs={{0,8},{8,16},{16,24},{24,32},{32,40},{40,48},{48,56},{56,64},{64,7... | collective-permute-start | bytes 61448 | tf_op jit(solution)/shard_map/ppermute | solution.py:572
  16.9 7.0 %shard_map.181 = (bf16[1024,256]{1,0:T(8,128)(2,1)S(1)}, bf16[1024,128]{1,0:T(8,128)(2,1)}, bf16[1024,128]{1,0:T(8,128)(2,1)S(1)}, bf16[1024,128]{1,0:T(8,128)(2...) custom-call(f32[2,2]{1,0:T(2,128)S(1)} %copy-done, ...), custom_call_target="tpu_custom_call" | custom-call | tf_op jit(solution)/shard_map/pallas_call | solution.py:543
  23.9 3.2 %collective-permute-start.3 = (bf16[208,128]{1,0:T(8,128)(2,1)S(1)}, bf16[208,128]{1,0:T(8,128)(2,1)S(1)}, u32[]{:S(2)}, u32[]{:S(2)}) collective-permute-start(bf16[208,128]{1,0:T(8,128)(2,1)S(1)} %get-tuple-element.39.own_ref), channel_id=1, source_target_pairs={{0,24},{8,0},{16,8},{24,16},{1,25},{9,1},{17,9},{25,17},{2,26},{10... | collective-permute-start | bytes 159752 | tf_op jit(solution)/shard_map/ppermute | solution.py:493
  28.5 4.1 %collective-permute-done.2.b2_ref = bf16[208,128]{1,0:T(8,128)(2,1)S(1)} collective-permute-done((bf16[208,128]{1,0:T(8,128)(2,1)S(1)}, bf16[208,128]{1,0:T(8,128)(2,1)S(1)}, u32[]{:S(2)}, u32[]{:S(2)}) %collective-permute-start.2) | collective-permute-done | bytes 53280 | tf_op jit(solution)/shard_map/ppermute | solution.py:493
  34.7 8.9 %all-to-all-start = ((bf16[8,208,128]{2,1,0:T(8,128)(2,1)}), bf16[8,208,128]{2,1,0:T(8,128)(2,1)S(1)}, u32[]{:S(2)}, u32[]{:S(2)}) async-start(bf16[8,208,128]{2,1,0:T(8,128)(2,1)} %get-tuple-element.40), calls=%async_computation | async-start | bytes 851968 | tf_op jit(solution)/shard_map/all_to_all | solution.py:617
  44.7 2.5 %collective-permute-start.11 = (bf16[2048,256]{1,0:T(8,128)(2,1)}, bf16[2048,256]{1,0:T(8,128)(2,1)}, u32[]{:S(2)}, u32[]{:S(2)}) collective-permute-start(bf16[2048,256]{1,0:T(8,128)(2,1)} %bitcast.10), channel_id=1, source_target_pairs={{0,1},{1,0},{2,3},{3,2},{4,5},{5,4},{6,7},{7,6},{8,9},{9,8},{10,11... | collective-permute-start | bytes 3145736 | tf_op jit(solution)/shard_map/ppermute | solution.py:493
  48.0 4.6 %shard_map.183.in_ref = f32[1024,256]{1,0:T(8,128)S(1)} custom-call(bf16[1024,256]{1,0:T(8,128)(2,1)S(1)} %get-tuple-element.41.xc_ref, bf16[1024,128]{1,0:T(8,128)(2,1)} %get-tuple-element.42.k1_ref, bf16[1024,128]{1,0:T(8,128)(2,1)S(1)} %get-tuple-element.43.q1_ref, bf16[1024,128]{1,0:T(8,128)(2,1)S(1)} %get-tuple-element.44.kq2_ref, ...), custom_call_target="tpu_custom_call" | custom-call | tf_op jit(solution)/shard_map/pallas_call | solution.py:543
  52.6 5.7 %all-to-all-done.rows_ref = bf16[8,208,128]{2,1,0:T(8,128)(2,1)S(1)} async-done(((bf16[8,208,128]{2,1,0:T(8,128)(2,1)}), bf16[8,208,128]{2,1,0:T(8,128)(2,1)S(1)}, u32[]{:S(2)}, u32[]{:S(2)}) %all-to-all-start) | async-done | bytes 426016 | tf_op jit(solution)/shard_map/all_to_all | solution.py:617
  58.3 4.1 %shard_map.184 = (bf16[512,256]{1,0:T(8,128)(2,1)S(1)}, bf16[512,256]{1,0:T(8,128)(2,1)S(1)}) custom-call(s32[4]{0:T(128)S(1)} %pad_add_fusion.y_ref.pos_ref, f32[1024,256]{1,0:T(8,128)S(1)} %shard_map.183.in_ref, bf16[1024,256]{1,0:T(8,128)(2,1)} %bitcast.25, bf16[1024,128]{1,0:T(8,128)(2,1)S(1)} %get-tuple-element.43.q1_ref, ...), custom_call_target="tpu_custom_call" | custom-call | tf_op jit(solution)/shard_map/pallas_call | solution.py:543
  62.4 2.6 %collective-permute-start.4 = (bf16[512,256]{1,0:T(8,128)(2,1)S(1)}, bf16[512,256]{1,0:T(8,128)(2,1)S(1)}, u32[]{:S(2)}, u32[]{:S(2)}) collective-permute-start(bf16[512,256]{1,0:T(8,128)(2,1)S(1)} %get-tuple-element.54), channel_id=1, source_target_pairs={{0,1},{1,0},{2,3},{3,2},{4,5},{5,4},{6,7},{7,6},{8,9},{9,8},{10,11... | collective-permute-start | bytes 786440 | tf_op jit(solution)/shard_map/ppermute | solution.py:493
  66.7 2.0 %collective-permute-start.8 = (bf16[512,256]{1,0:T(8,128)(2,1)S(1)}, bf16[512,256]{1,0:T(8,128)(2,1)S(1)}, u32[]{:S(2)}, u32[]{:S(2)}) collective-permute-start(bf16[512,256]{1,0:T(8,128)(2,1)S(1)} %collective-permute-done.4.refs_1_), channel_id=1, source_target_pairs={{0,6},{2,0},{4,2},{6,4},{1,7},{3,1},{5,3},{7,5},{8,14},{10,8},{12,... | collective-permute-start | bytes 786440 | tf_op jit(solution)/shard_map/ppermute | solution.py:493
  70.4 3.6 %collective-permute-done.5.refs_2_ = bf16[512,256]{1,0:T(8,128)(2,1)S(1)} collective-permute-done((bf16[512,256]{1,0:T(8,128)(2,1)S(1)}, bf16[512,256]{1,0:T(8,128)(2,1)S(1)}, u32[]{:S(2)}, u32[]{:S(2)}) %collective-permute-start.5) | collective-permute-done | bytes 262176 | tf_op jit(solution)/shard_map/ppermute | solution.py:493
  74.2 3.3 %collective-permute-start.10 = (bf16[512,256]{1,0:T(8,128)(2,1)S(1)}, bf16[512,256]{1,0:T(8,128)(2,1)S(1)}, u32[]{:S(2)}, u32[]{:S(2)}) collective-permute-start(bf16[512,256]{1,0:T(8,128)(2,1)S(1)} %collective-permute-done.8.refs_5_), channel_id=1, source_target_pairs={{0,6},{2,0},{4,2},{6,4},{1,7},{3,1},{5,3},{7,5},{8,14},{10,8},{12,... | collective-permute-start | bytes 786440 | tf_op jit(solution)/shard_map/ppermute | solution.py:493
  77.5 2.9 %maximum_select_fusion.refs_8_ = bf16[2048,512]{1,0:T(8,128)(2,1)S(1)} fusion(bf16[2048,256]{1,0:T(8,128)(2,1)} %collective-permute-done.11, bf16[2048,256]{1,0:T(8,128)(2,1)} %bitcast.10, pred[]{:T(512)S(6)} %eq.4), kind=kLoop, calls=%fused_computation | loop fusion | flops 9437184 | bytes 4194305 | tf_op jit(solution)/shard_map/jit(_where)/select_n | solution.py:643
  80.5 4.7 %collective-permute-done.9.refs_6_ = bf16[512,256]{1,0:T(8,128)(2,1)S(1)} collective-permute-done((bf16[512,256]{1,0:T(8,128)(2,1)S(1)}, bf16[512,256]{1,0:T(8,128)(2,1)S(1)}, u32[]{:S(2)}, u32[]{:S(2)}) %collective-permute-start.9) | collective-permute-done | bytes 262176 | tf_op jit(solution)/shard_map/ppermute | solution.py:493
  85.2 2.1 %shard_map.185 = (bf16[256,512]{1,0:T(8,128)(2,1)S(1)}, bf16[256,512]{1,0:T(8,128)(2,1)S(1)}) custom-call(s32[4]{0:T(128)S(1)} %pad_add_fusion.y_ref.pos_ref, bf16[512,256]{1,0:T(8,128)(2,1)S(1)} %get-tuple-element.53.refs_0_, bf16[512,256]{1,0:T(8,128)(2,1)S(1)} %collective-permute-done.4.refs_1_, bf16[512,256]{1,0:T(8,128)(2,1)S(1)} %collective-permute-done.5.refs_2_, ...), custom_call_target="tpu_custom_call" | custom-call | tf_op jit(solution)/shard_map/pallas_call | solution.py:543
  88.3 2.7 %collective-permute-start.17 = (bf16[256,512]{1,0:T(8,128)(2,1)S(1)}, bf16[256,512]{1,0:T(8,128)(2,1)S(1)}, u32[]{:S(2)}, u32[]{:S(2)}) collective-permute-start(bf16[256,512]{1,0:T(8,128)(2,1)S(1)} %get-tuple-element.58.refs_4_.sb_ref), channel_id=1, source_target_pairs={{0,6},{2,0},{4,2},{6,4},{1,7},{3,1},{5,3},{7,5},{8,14},{10,8},{12,... | collective-permute-start | bytes 786440 | tf_op jit(solution)/shard_map/ppermute | solution.py:493
  92.4 4.1 %collective-permute-done.13.refs_1_ = bf16[256,512]{1,0:T(8,128)(2,1)S(1)} collective-permute-done((bf16[256,512]{1,0:T(8,128)(2,1)S(1)}, bf16[256,512]{1,0:T(8,128)(2,1)S(1)}, u32[]{:S(2)}, u32[]{:S(2)}) %collective-permute-start.13) | collective-permute-done | bytes 262176 | tf_op jit(solution)/shard_map/ppermute | solution.py:493
  96.5 2.7 %collective-permute-start.18 = (bf16[256,512]{1,0:T(8,128)(2,1)S(1)}, bf16[256,512]{1,0:T(8,128)(2,1)S(1)}, u32[]{:S(2)}, u32[]{:S(2)}) collective-permute-start(bf16[256,512]{1,0:T(8,128)(2,1)S(1)} %collective-permute-done.17.refs_6_), channel_id=1, source_target_pairs={{0,6},{2,0},{4,2},{6,4},{1,7},{3,1},{5,3},{7,5},{8,14},{10,8},{12,... | collective-permute-start | bytes 786440 | tf_op jit(solution)/shard_map/ppermute | solution.py:493
  99.2 1.9 %collective-permute-done.14.refs_2_ = bf16[256,512]{1,0:T(8,128)(2,1)S(1)} collective-permute-done((bf16[256,512]{1,0:T(8,128)(2,1)S(1)}, bf16[256,512]{1,0:T(8,128)(2,1)S(1)}, u32[]{:S(2)}, u32[]{:S(2)}) %collective-permute-start.14) | collective-permute-done | bytes 262176 | tf_op jit(solution)/shard_map/ppermute | solution.py:493
  102.1 5.6 %collective-permute-done.15.refs_3_ = bf16[256,512]{1,0:T(8,128)(2,1)S(1)} collective-permute-done((bf16[256,512]{1,0:T(8,128)(2,1)S(1)}, bf16[256,512]{1,0:T(8,128)(2,1)S(1)}, u32[]{:S(2)}, u32[]{:S(2)}) %collective-permute-start.15) | collective-permute-done | bytes 262176 | tf_op jit(solution)/shard_map/ppermute | solution.py:493
  109.3 3.9 %all-gather.2.cloned.1.call-done = bf16[4096,1920]{1,0:T(8,128)(2,1)} async-done(((bf16[64,1920]{1,0:T(8,128)(2,1)}), bf16[4096,1920]{1,0:T(8,128)(2,1)}) %all-gather.2.cloned.1.call-update) | async-done | bytes 15728656 | tf_op jit(solution)/shard_map/all_gather | solution.py:567
  113.2 9.5 %shard_map.187 = (bf16[256,512]{1,0:T(8,128)(2,1)S(1)}, bf16[256,512]{1,0:T(8,128)(2,1)S(1)}, bf16[512,1280]{1,0:T(8,128)(2,1)S(1)}, bf16[32,64,1280]{2,1,0:T(8,128)(2,1)S(1)}) custom-call(s32[4]{0:T(128)S(1)} %pad_add_fusion.y_ref.pos_ref, bf16[512,2048]{1,0:T(8,128)(2,1)S(1)} %shard_map.186.normed, bf16[32,2,64,1920]{3,2,1,0:T(8,128)(2,1)} %bitcast.22), custom_call_target="tpu_custom_call" | custom-call | tf_op jit(solution)/shard_map/pallas_call | solution.py:543
  125.7 2.8 %shard_map.188 = (bf16[256,512]{1,0:T(8,128)(2,1)S(1)}, bf16[256,512]{1,0:T(8,128)(2,1)S(1)}, bf16[256,512]{1,0:T(8,128)(2,1)S(1)}, bf16[256,512]{1,0:T(8,128)(2...) custom-call(s32[4]{0:T(128)S(1)} %pad_add_fusion.y_ref.pos_ref, ...), custom_call_target="tpu_custom_call" | custom-call | tf_op jit(solution)/shard_map/pallas_call | solution.py:543
  130.1 1.8 %collective-permute-done.19 = bf16[256,512]{1,0:T(8,128)(2,1)S(1)} collective-permute-done((bf16[256,512]{1,0:T(8,128)(2,1)S(1)}, bf16[256,512]{1,0:T(8,128)(2,1)S(1)}, u32[]{:S(2)}, u32[]{:S(2)}) %collective-permute-start.19) | collective-permute-done | bytes 262176 | tf_op jit(solution)/shard_map/ppermute | solution.py:493
  132.1 2.7 %collective-permute-start.24 = (bf16[256,512]{1,0:T(8,128)(2,1)S(1)}, bf16[256,512]{1,0:T(8,128)(2,1)S(1)}, u32[]{:S(2)}, u32[]{:S(2)}) collective-permute-start(bf16[256,512]{1,0:T(8,128)(2,1)S(1)} %add_convert_fusion), channel_id=1, source_target_pairs={{0,6},{2,0},{4,2},{6,4},{1,7},{3,1},{5,3},{7,5},{8,14},{10,8},{12,... | collective-permute-start | bytes 786440 | tf_op jit(solution)/shard_map/ppermute | solution.py:493
  134.9 2.3 %collective-permute-done.21.ra_ref = bf16[256,512]{1,0:T(8,128)(2,1)S(1)} collective-permute-done((bf16[256,512]{1,0:T(8,128)(2,1)S(1)}, bf16[256,512]{1,0:T(8,128)(2,1)S(1)}, u32[]{:S(2)}, u32[]{:S(2)}) %collective-permute-start.21) | collective-permute-done | bytes 262176 | tf_op jit(solution)/shard_map/ppermute | solution.py:493
  137.8 5.6 %collective-permute-done.20.la_ref = bf16[256,512]{1,0:T(8,128)(2,1)S(1)} collective-permute-done((bf16[256,512]{1,0:T(8,128)(2,1)S(1)}, bf16[256,512]{1,0:T(8,128)(2,1)S(1)}, u32[]{:S(2)}, u32[]{:S(2)}) %collective-permute-start.20) | collective-permute-done | bytes 262176 | tf_op jit(solution)/shard_map/ppermute | solution.py:493
  144.1 2.1 %collective-permute-start.25 = (bf16[512,256]{1,0:T(8,128)(2,1)S(1)}, bf16[512,256]{1,0:T(8,128)(2,1)S(1)}, u32[]{:S(2)}, u32[]{:S(2)}) collective-permute-start(bf16[512,256]{1,0:T(8,128)(2,1)S(1)} %shard_map.190), channel_id=1, source_target_pairs={{0,1},{1,0},{2,3},{3,2},{4,5},{5,4},{6,7},{7,6},{8,9},{9,8},{10,11... | collective-permute-start | bytes 786440 | tf_op jit(solution)/shard_map/ppermute | solution.py:493
  (55 shorter events, 23.9 us)
Async XLA Ops:
  6.5 10.3 %copy-start = (f32[2,2]{1,0:T(2,128)S(1)}, f32[2,2]{1,0:T(2,128)}, u32[]{:S(2)}) copy-start(f32[2,2]{1,0:T(2,128)} %rate_ref.1) | copy-start | bytes 52
  6.5 106.7 %all-gather.2.cloned.1.call-start = ((), (), s32[]{:S(2)}) async-start(), calls=%async_computation.1 | async-start | bytes 15974400 | tf_op jit(solution)/shard_map/all_gather | solution.py:567
  10.2 33.4 %copy-start.1 = (bf16[2,1024,256]{2,1,0:T(8,128)(2,1)S(1)}, bf16[2,1024,256]{2,1,0:T(8,128)(2,1)}, u32[]{:S(2)}) copy-start(bf16[2,1024,256]{2,1,0:T(8,128)(2,1)} %param.32) | copy-start | bytes 3145732
  11.8 5.1 %collective-permute-start = (bf16[16,640]{1,0:T(8,128)(2,1)}, bf16[16,640]{1,0:T(8,128)(2,1)S(1)}, u32[]{:S(2)}, u32[]{:S(2)}) collective-permute-start(bf16[16,640]{1,0:T(8,128)(2,1)} %pack_rim.1), channel_id=1, source_target_pairs={{0,8},{8,16},{16,24},{24,32},{32,40},{40,48},{48,56},{56,64},{64,7... | collective-permute-start | bytes 61448 | tf_op jit(solution)/shard_map/ppermute | solution.py:572
  16.9 30.3 %copy-start.3 = (bf16[1024,2,128]{2,1,0:T(2,128)(2,1)S(1)}, bf16[1024,2,128]{2,1,0:T(2,128)(2,1)}, u32[]{:S(2)}) copy-start(bf16[1024,2,128]{2,1,0:T(2,128)(2,1)} %param.20) | copy-start | bytes 1572868
  23.9 4.6 %collective-permute-start.3 = (bf16[208,128]{1,0:T(8,128)(2,1)S(1)}, bf16[208,128]{1,0:T(8,128)(2,1)S(1)}, u32[]{:S(2)}, u32[]{:S(2)}) collective-permute-start(bf16[208,128]{1,0:T(8,128)(2,1)S(1)} %get-tuple-element.39.own_ref), channel_id=1, source_target_pairs={{0,24},{8,0},{16,8},{24,16},{1,25},{9,1},{17,9},{25,17},{2,26},{10... | collective-permute-start | bytes 159752 | tf_op jit(solution)/shard_map/ppermute | solution.py:493
  27.0 5.5 %collective-permute-start.2 = (bf16[208,128]{1,0:T(8,128)(2,1)S(1)}, bf16[208,128]{1,0:T(8,128)(2,1)S(1)}, u32[]{:S(2)}, u32[]{:S(2)}) collective-permute-start(bf16[208,128]{1,0:T(8,128)(2,1)S(1)} %get-tuple-element.39.own_ref), channel_id=1, source_target_pairs={{0,16},{8,24},{16,0},{24,8},{1,17},{9,25},{17,1},{25,9},{2,18},{10... | collective-permute-start | bytes 159752 | tf_op jit(solution)/shard_map/ppermute | solution.py:493
  27.4 6.0 %collective-permute-start.1 = (bf16[208,128]{1,0:T(8,128)(2,1)S(1)}, bf16[208,128]{1,0:T(8,128)(2,1)S(1)}, u32[]{:S(2)}, u32[]{:S(2)}) collective-permute-start(bf16[208,128]{1,0:T(8,128)(2,1)S(1)} %get-tuple-element.39.own_ref), channel_id=1, source_target_pairs={{0,8},{8,16},{16,24},{24,0},{1,9},{9,17},{17,25},{25,1},{2,10},{10... | collective-permute-start | bytes 159752 | tf_op jit(solution)/shard_map/ppermute | solution.py:493
  34.7 23.6 %all-to-all-start = ((bf16[8,208,128]{2,1,0:T(8,128)(2,1)}), bf16[8,208,128]{2,1,0:T(8,128)(2,1)S(1)}, u32[]{:S(2)}, u32[]{:S(2)}) async-start(bf16[8,208,128]{2,1,0:T(8,128)(2,1)} %get-tuple-element.40), calls=%async_computation | async-start | bytes 851968 | tf_op jit(solution)/shard_map/all_to_all | solution.py:617
  44.7 32.8 %collective-permute-start.11 = (bf16[2048,256]{1,0:T(8,128)(2,1)}, bf16[2048,256]{1,0:T(8,128)(2,1)}, u32[]{:S(2)}, u32[]{:S(2)}) collective-permute-start(bf16[2048,256]{1,0:T(8,128)(2,1)} %bitcast.10), channel_id=1, source_target_pairs={{0,1},{1,0},{2,3},{3,2},{4,5},{5,4},{6,7},{7,6},{8,9},{9,8},{10,11... | collective-permute-start | bytes 3145736 | tf_op jit(solution)/shard_map/ppermute | solution.py:493
  52.6 12.4 %copy-start.2 = (bf16[1024,256]{1,0:T(8,128)(2,1)S(1)}, bf16[1024,256]{1,0:T(8,128)(2,1)}, u32[]{:S(2)}) copy-start(bf16[1024,256]{1,0:T(8,128)(2,1)} %param.33) | copy-start | bytes 1572868
  62.4 4.3 %collective-permute-start.4 = (bf16[512,256]{1,0:T(8,128)(2,1)S(1)}, bf16[512,256]{1,0:T(8,128)(2,1)S(1)}, u32[]{:S(2)}, u32[]{:S(2)}) collective-permute-start(bf16[512,256]{1,0:T(8,128)(2,1)S(1)} %get-tuple-element.54), channel_id=1, source_target_pairs={{0,1},{1,0},{2,3},{3,2},{4,5},{5,4},{6,7},{7,6},{8,9},{9,8},{10,11... | collective-permute-start | bytes 786440 | tf_op jit(solution)/shard_map/ppermute | solution.py:493
  65.0 3.7 %collective-permute-start.12 = (bf16[512,256]{1,0:T(8,128)(2,1)S(1)}, bf16[512,256]{1,0:T(8,128)(2,1)S(1)}, u32[]{:S(2)}, u32[]{:S(2)}) collective-permute-start(bf16[512,256]{1,0:T(8,128)(2,1)S(1)} %get-tuple-element.70), channel_id=1, source_target_pairs={{0,1},{1,0},{2,3},{3,2},{4,5},{5,4},{6,7},{7,6},{8,9},{9,8},{10,11... | collective-permute-start | bytes 786440 | tf_op jit(solution)/shard_map/ppermute | solution.py:493
  65.1 8.8 %collective-permute-start.5 = (bf16[512,256]{1,0:T(8,128)(2,1)S(1)}, bf16[512,256]{1,0:T(8,128)(2,1)S(1)}, u32[]{:S(2)}, u32[]{:S(2)}) collective-permute-start(bf16[512,256]{1,0:T(8,128)(2,1)S(1)} %get-tuple-element.53.refs_0_), channel_id=1, source_target_pairs={{0,2},{2,4},{4,6},{6,0},{1,3},{3,5},{5,7},{7,1},{8,10},{10,12},{12... | collective-permute-start | bytes 786440 | tf_op jit(solution)/shard_map/ppermute | solution.py:493
  66.7 7.5 %collective-permute-start.8 = (bf16[512,256]{1,0:T(8,128)(2,1)S(1)}, bf16[512,256]{1,0:T(8,128)(2,1)S(1)}, u32[]{:S(2)}, u32[]{:S(2)}) collective-permute-start(bf16[512,256]{1,0:T(8,128)(2,1)S(1)} %collective-permute-done.4.refs_1_), channel_id=1, source_target_pairs={{0,6},{2,0},{4,2},{6,4},{1,7},{3,1},{5,3},{7,5},{8,14},{10,8},{12,... | collective-permute-start | bytes 786440 | tf_op jit(solution)/shard_map/ppermute | solution.py:493
  68.8 11.6 %collective-permute-start.7 = (bf16[512,256]{1,0:T(8,128)(2,1)S(1)}, bf16[512,256]{1,0:T(8,128)(2,1)S(1)}, u32[]{:S(2)}, u32[]{:S(2)}) collective-permute-start(bf16[512,256]{1,0:T(8,128)(2,1)S(1)} %get-tuple-element.53.refs_0_), channel_id=1, source_target_pairs={{0,6},{2,0},{4,2},{6,4},{1,7},{3,1},{5,3},{7,5},{8,14},{10,8},{12,... | collective-permute-start | bytes 786440 | tf_op jit(solution)/shard_map/ppermute | solution.py:493
  69.4 11.0 %collective-permute-start.6 = (bf16[512,256]{1,0:T(8,128)(2,1)S(1)}, bf16[512,256]{1,0:T(8,128)(2,1)S(1)}, u32[]{:S(2)}, u32[]{:S(2)}) collective-permute-start(bf16[512,256]{1,0:T(8,128)(2,1)S(1)} %collective-permute-done.4.refs_1_), channel_id=1, source_target_pairs={{0,2},{2,4},{4,6},{6,0},{1,3},{3,5},{5,7},{7,1},{8,10},{10,12},{12... | collective-permute-start | bytes 786440 | tf_op jit(solution)/shard_map/ppermute | solution.py:493
  73.9 11.2 %collective-permute-start.9 = (bf16[512,256]{1,0:T(8,128)(2,1)S(1)}, bf16[512,256]{1,0:T(8,128)(2,1)S(1)}, u32[]{:S(2)}, u32[]{:S(2)}) collective-permute-start(bf16[512,256]{1,0:T(8,128)(2,1)S(1)} %collective-permute-done.5.refs_2_), channel_id=1, source_target_pairs={{0,2},{2,4},{4,6},{6,0},{1,3},{3,5},{5,7},{7,1},{8,10},{10,12},{12... | collective-permute-start | bytes 786440 | tf_op jit(solution)/shard_map/ppermute | solution.py:493
  74.2 11.0 %collective-permute-start.10 = (bf16[512,256]{1,0:T(8,128)(2,1)S(1)}, bf16[512,256]{1,0:T(8,128)(2,1)S(1)}, u32[]{:S(2)}, u32[]{:S(2)}) collective-permute-start(bf16[512,256]{1,0:T(8,128)(2,1)S(1)} %collective-permute-done.8.refs_5_), channel_id=1, source_target_pairs={{0,6},{2,0},{4,2},{6,4},{1,7},{3,1},{5,3},{7,5},{8,14},{10,8},{12,... | collective-permute-start | bytes 786440 | tf_op jit(solution)/shard_map/ppermute | solution.py:493
  87.3 9.3 %collective-permute-start.13 = (bf16[256,512]{1,0:T(8,128)(2,1)S(1)}, bf16[256,512]{1,0:T(8,128)(2,1)S(1)}, u32[]{:S(2)}, u32[]{:S(2)}) collective-permute-start(bf16[256,512]{1,0:T(8,128)(2,1)S(1)} %get-tuple-element.57.refs_0_.sa_ref), channel_id=1, source_target_pairs={{0,2},{2,4},{4,6},{6,0},{1,3},{3,5},{5,7},{7,1},{8,10},{10,12},{12... | collective-permute-start | bytes 786440 | tf_op jit(solution)/shard_map/ppermute | solution.py:493
  88.3 8.3 %collective-permute-start.17 = (bf16[256,512]{1,0:T(8,128)(2,1)S(1)}, bf16[256,512]{1,0:T(8,128)(2,1)S(1)}, u32[]{:S(2)}, u32[]{:S(2)}) collective-permute-start(bf16[256,512]{1,0:T(8,128)(2,1)S(1)} %get-tuple-element.58.refs_4_.sb_ref), channel_id=1, source_target_pairs={{0,6},{2,0},{4,2},{6,4},{1,7},{3,1},{5,3},{7,5},{8,14},{10,8},{12,... | collective-permute-start | bytes 786440 | tf_op jit(solution)/shard_map/ppermute | solution.py:493
  90.9 10.2 %collective-permute-start.14 = (bf16[256,512]{1,0:T(8,128)(2,1)S(1)}, bf16[256,512]{1,0:T(8,128)(2,1)S(1)}, u32[]{:S(2)}, u32[]{:S(2)}) collective-permute-start(bf16[256,512]{1,0:T(8,128)(2,1)S(1)} %get-tuple-element.57.refs_0_.sa_ref), channel_id=1, source_target_pairs={{0,6},{2,0},{4,2},{6,4},{1,7},{3,1},{5,3},{7,5},{8,14},{10,8},{12,... | collective-permute-start | bytes 786440 | tf_op jit(solution)/shard_map/ppermute | solution.py:493
  92.3 9.8 %collective-permute-start.16 = (bf16[256,512]{1,0:T(8,128)(2,1)S(1)}, bf16[256,512]{1,0:T(8,128)(2,1)S(1)}, u32[]{:S(2)}, u32[]{:S(2)}) collective-permute-start(bf16[256,512]{1,0:T(8,128)(2,1)S(1)} %get-tuple-element.58.refs_4_.sb_ref), channel_id=1, source_target_pairs={{0,2},{2,4},{4,6},{6,0},{1,3},{3,5},{5,7},{7,1},{8,10},{10,12},{12... | collective-permute-start | bytes 786440 | tf_op jit(solution)/shard_map/ppermute | solution.py:493
  96.5 11.2 %collective-permute-start.15 = (bf16[256,512]{1,0:T(8,128)(2,1)S(1)}, bf16[256,512]{1,0:T(8,128)(2,1)S(1)}, u32[]{:S(2)}, u32[]{:S(2)}) collective-permute-start(bf16[256,512]{1,0:T(8,128)(2,1)S(1)} %collective-permute-done.13.refs_1_), channel_id=1, source_target_pairs={{0,2},{2,4},{4,6},{6,0},{1,3},{3,5},{5,7},{7,1},{8,10},{10,12},{12... | collective-permute-start | bytes 786440 | tf_op jit(solution)/shard_map/ppermute | solution.py:493
  96.5 11.2 %collective-permute-start.18 = (bf16[256,512]{1,0:T(8,128)(2,1)S(1)}, bf16[256,512]{1,0:T(8,128)(2,1)S(1)}, u32[]{:S(2)}, u32[]{:S(2)}) collective-permute-start(bf16[256,512]{1,0:T(8,128)(2,1)S(1)} %collective-permute-done.17.refs_6_), channel_id=1, source_target_pairs={{0,6},{2,0},{4,2},{6,4},{1,7},{3,1},{5,3},{7,5},{8,14},{10,8},{12,... | collective-permute-start | bytes 786440 | tf_op jit(solution)/shard_map/ppermute | solution.py:493
  122.8 9.1 %collective-permute-start.19 = (bf16[256,512]{1,0:T(8,128)(2,1)S(1)}, bf16[256,512]{1,0:T(8,128)(2,1)S(1)}, u32[]{:S(2)}, u32[]{:S(2)}) collective-permute-start(bf16[256,512]{1,0:T(8,128)(2,1)S(1)} %get-tuple-element.63), channel_id=1, source_target_pairs={{0,2},{2,4},{4,6},{6,0},{1,3},{3,5},{5,7},{7,1},{8,10},{10,12},{12... | collective-permute-start | bytes 786440 | tf_op jit(solution)/shard_map/ppermute | solution.py:493
  124.3 7.8 %collective-permute-start.23 = (bf16[256,512]{1,0:T(8,128)(2,1)S(1)}, bf16[256,512]{1,0:T(8,128)(2,1)S(1)}, u32[]{:S(2)}, u32[]{:S(2)}) collective-permute-start(bf16[256,512]{1,0:T(8,128)(2,1)S(1)} %get-tuple-element.68), channel_id=1, source_target_pairs={{0,6},{2,0},{4,2},{6,4},{1,7},{3,1},{5,3},{7,5},{8,14},{10,8},{12,... | collective-permute-start | bytes 786440 | tf_op jit(solution)/shard_map/ppermute | solution.py:493
  128.5 8.7 %collective-permute-start.21 = (bf16[256,512]{1,0:T(8,128)(2,1)S(1)}, bf16[256,512]{1,0:T(8,128)(2,1)S(1)}, u32[]{:S(2)}, u32[]{:S(2)}) collective-permute-start(bf16[256,512]{1,0:T(8,128)(2,1)S(1)} %get-tuple-element.64), channel_id=1, source_target_pairs={{0,6},{2,0},{4,2},{6,4},{1,7},{3,1},{5,3},{7,5},{8,14},{10,8},{12,... | collective-permute-start | bytes 786440 | tf_op jit(solution)/shard_map/ppermute | solution.py:493
  129.8 8.0 %collective-permute-start.22 = (bf16[256,512]{1,0:T(8,128)(2,1)S(1)}, bf16[256,512]{1,0:T(8,128)(2,1)S(1)}, u32[]{:S(2)}, u32[]{:S(2)}) collective-permute-start(bf16[256,512]{1,0:T(8,128)(2,1)S(1)} %get-tuple-element.66), channel_id=1, source_target_pairs={{0,2},{2,4},{4,6},{6,0},{1,3},{3,5},{5,7},{7,1},{8,10},{10,12},{12... | collective-permute-start | bytes 786440 | tf_op jit(solution)/shard_map/ppermute | solution.py:493
  131.9 11.4 %collective-permute-start.20 = (bf16[256,512]{1,0:T(8,128)(2,1)S(1)}, bf16[256,512]{1,0:T(8,128)(2,1)S(1)}, u32[]{:S(2)}, u32[]{:S(2)}) collective-permute-start(bf16[256,512]{1,0:T(8,128)(2,1)S(1)} %add_convert_fusion.1), channel_id=1, source_target_pairs={{0,2},{2,4},{4,6},{6,0},{1,3},{3,5},{5,7},{7,1},{8,10},{10,12},{12... | collective-permute-start | bytes 786440 | tf_op jit(solution)/shard_map/ppermute | solution.py:493
  132.1 11.3 %collective-permute-start.24 = (bf16[256,512]{1,0:T(8,128)(2,1)S(1)}, bf16[256,512]{1,0:T(8,128)(2,1)S(1)}, u32[]{:S(2)}, u32[]{:S(2)}) collective-permute-start(bf16[256,512]{1,0:T(8,128)(2,1)S(1)} %add_convert_fusion), channel_id=1, source_target_pairs={{0,6},{2,0},{4,2},{6,4},{1,7},{3,1},{5,3},{7,5},{8,14},{10,8},{12,... | collective-permute-start | bytes 786440 | tf_op jit(solution)/shard_map/ppermute | solution.py:493
  144.1 3.2 %collective-permute-start.25 = (bf16[512,256]{1,0:T(8,128)(2,1)S(1)}, bf16[512,256]{1,0:T(8,128)(2,1)S(1)}, u32[]{:S(2)}, u32[]{:S(2)}) collective-permute-start(bf16[512,256]{1,0:T(8,128)(2,1)S(1)} %shard_map.190), channel_id=1, source_target_pairs={{0,1},{1,0},{2,3},{3,2},{4,5},{5,4},{6,7},{7,6},{8,9},{9,8},{10,11... | collective-permute-start | bytes 786440 | tf_op jit(solution)/shard_map/ppermute | solution.py:493
Sparse Core Ops, SparseCore 0:
  10.1 103.1 all-gather.1
